TPU v7x, 32 devices: a whole 2x2x4 slice. The times are simulated.
32 devices in a mesh: ep: 8 (over z, x), tp: 4 (over y, core).
Axes of the slice: x: 2, y: 2, z: 4, core: 2. Of those that a mesh axis runs over, the one named last changes fastest.
Arguments:
- query_latent: bfloat16 [1024, 512], P('ep'), may hold values from -6 to 6
- key_latent: bfloat16 [1024, 256], P('ep'), may hold values from -6 to 6
- rope_key: bfloat16 [1024, 64], P('ep'), may hold values from -500 to 500
- query_gain: float32 [512], replicated, may hold values from 0.1 to 1.9
- key_gain: float32 [256], replicated, may hold values from 0.1 to 1.9
- w_query: bfloat16 [512, 1024], P(None, 'tp'), may hold values from -0.25 to 0.25
- w_query_rope: bfloat16 [512, 512], P(None, 'tp'), may hold values from -0.25 to 0.25
- w_key: bfloat16 [256, 1024], P(None, 'tp'), may hold values from -0.375 to 0.375
- w_value: bfloat16 [256, 1024], P(None, 'tp'), may hold values from -0.375 to 0.375
- w_out: bfloat16 [1024, 2048], P('tp'), may hold values from -1.796875 to 1.796875
- tokens_b: bfloat16 [4096, 2048], P('ep'), may hold values from -6 to 6
- ffn_gain: float32 [2048], replicated, may hold values from 0.1 to 1.9
- route_expert: int32 [4096, 2], P('ep'), may hold values from 0 to 7, as said below
- route_weight: float32 [4096, 2], P('ep'), may hold values from 0.2 to 1
- w_gate: bfloat16 [8, 2048, 1024], P('ep', None, 'tp'), may hold values from -0.125 to 0.125
- w_up: bfloat16 [8, 2048, 1024], P('ep', None, 'tp'), may hold values from -0.125 to 0.125
- w_down: bfloat16 [8, 1024, 2048], P('ep', 'tp'), may hold values from -0.1875 to 0.1875
Outputs:
- mixer_out: bfloat16 [1024, 2048], P(('ep', 'tp'))
- moe_out: bfloat16 [4096, 2048], P('ep', 'tp')
Inputs may be any that keep to these rules, and one draw needn't show every extreme that they name: `route_expert`: expert e belongs to group e // 2. A row's 2 experts differ and lie in one group. Among the rows of one device along ep, every group is named by exactly 128 rows and every expert is named exactly 128 times.
All inputs are finite; a program needn't handle non-finite values.
Results may differ from a plain program's by a relative error of at most 0.013.
The roundings to bfloat16 on the way count: a program that leaves them out, or rounds other values in their place, can miss the bound.
Values may be sent and summed in bfloat16 or wider, within the bound.
A program may use at most 64 MiB of HBM per device.

v0:
```python
import math

import jax
import jax.numpy as jnp
from jax import lax
from jax.experimental import pallas as pl
from jax.experimental.pallas import tpu as pltpu
from jax.sharding import PartitionSpec as P

NOPE = 128
ROPE = 64
VDIM = 128
GRID_W = 64
TOPK = 2
GROUPS = 4
MESH = pl.DeviceIdType.MESH
SPLIT_NUM, SPLIT_DEN = 1, 8
JOIN_FIRST = ()


epsilon = 1e-06
rotary_base = 10000.0
neg_large = -1e30


def rms_scale(values_in, gain):
    widened = values_in.astype(jnp.float32)
    normed = widened * lax.rsqrt(jnp.mean(widened * widened, axis=-1, keepdims=True) + epsilon)
    return (normed * gain).astype(jnp.bfloat16)


def rotary_tables(positions):
    half_width = ROPE // 2
    inverse = rotary_base ** (-jnp.arange(0, half_width, 2, dtype=jnp.float32) / half_width)
    grid_row = (positions // GRID_W).astype(jnp.float32)
    grid_col = (positions % GRID_W).astype(jnp.float32)
    angle = jnp.concatenate([grid_row[:, None] * inverse, grid_col[:, None] * inverse], axis=-1)
    return (jnp.cos(angle), jnp.sin(angle))


def rotate(values_in, cosine, sine):
    even_part = values_in[..., 0::2]
    odd_part = values_in[..., 1::2]
    turned = jnp.stack(
        [even_part * cosine - odd_part * sine, even_part * sine + odd_part * cosine], axis=-1
    )
    return turned.reshape(values_in.shape)


def fold_blocks(carry, members, step_fn):
    piece_rows = members[0].shape[0]
    block_rows = math.gcd(piece_rows, 1024)
    if block_rows == piece_rows:
        return step_fn(carry, members)
    stacked = tuple(
        (
            member.reshape((piece_rows // block_rows, block_rows) + member.shape[1:])
            for member in members
        )
    )

    def scan_step(inner_carry, blocks):
        return (step_fn(inner_carry, blocks), None)

    result, unused = lax.scan(scan_step, carry, stacked)
    return result


def mixer_half(
    query_latent,
    key_latent,
    rope_key,
    query_gain,
    key_gain,
    w_query,
    w_query_rope,
    w_key,
    w_value,
    w_out,
):
    tok_rows = query_latent.shape[0]
    local_heads = w_query.shape[1] // NOPE
    positions = lax.axis_index("ep") * tok_rows + jnp.arange(tok_rows, dtype=jnp.int32)
    cosine, sine = rotary_tables(positions)
    query_normed = rms_scale(query_latent, query_gain)
    query_nope = jnp.dot(query_normed, w_query, preferred_element_type=jnp.float32).astype(
        jnp.bfloat16
    )
    query_nope = query_nope.reshape(tok_rows, local_heads, NOPE)
    query_rot = jnp.dot(query_normed, w_query_rope, preferred_element_type=jnp.float32)
    query_rot = rotate(
        query_rot.reshape(tok_rows, local_heads, ROPE), cosine[:, None, :], sine[:, None, :]
    )
    query_rot = query_rot.astype(jnp.bfloat16)
    key_rot = rotate(rope_key.astype(jnp.float32), cosine, sine).astype(jnp.bfloat16)
    score_scale = (NOPE + ROPE) ** (-0.5)

    def expand(latent_rows):
        latent_count = latent_rows.shape[0]
        key_normed = rms_scale(latent_rows, key_gain)
        key_nope = jnp.dot(key_normed, w_key, preferred_element_type=jnp.float32).astype(
            jnp.bfloat16
        )
        value_rows = jnp.dot(key_normed, w_value, preferred_element_type=jnp.float32).astype(
            jnp.bfloat16
        )
        return (
            key_nope.reshape(latent_count, local_heads, NOPE),
            value_rows.reshape(latent_count, local_heads, VDIM),
        )

    def attend_block(carry, key_nope, value_rows, key_turn):
        run_max, run_total, run_acc = carry
        scores = jnp.einsum(
            "qhd,khd->hqk", query_nope, key_nope, preferred_element_type=jnp.float32
        )
        scores = scores + jnp.einsum(
            "qhd,kd->hqk", query_rot, key_turn, preferred_element_type=jnp.float32
        )
        scores = scores * score_scale
        new_max = jnp.maximum(run_max, jnp.max(scores, axis=-1))
        correction = jnp.exp(run_max - new_max)
        weights = jnp.exp(scores - new_max[..., None])
        new_total = run_total * correction + jnp.sum(weights, axis=-1)
        added = jnp.einsum(
            "hqk,khd->qhd",
            weights.astype(jnp.bfloat16),
            value_rows,
            preferred_element_type=jnp.float32,
        )
        new_acc = run_acc * jnp.transpose(correction)[..., None] + added
        return (new_max, new_total, new_acc)

    def step_latent(carry, blocks):
        key_nope, value_rows = expand(blocks[0])
        return attend_block(carry, key_nope, value_rows, blocks[1])

    initial = (
        jnp.full((local_heads, tok_rows), neg_large, jnp.float32),
        jnp.zeros((local_heads, tok_rows), jnp.float32),
        jnp.zeros((tok_rows, local_heads, VDIM), jnp.float32),
    )
    gathered = lax.all_gather(
        jnp.concatenate([key_latent, key_rot], axis=1), "ep", axis=0, tiled=True
    )
    rank = key_latent.shape[1]
    final = fold_blocks(initial, (gathered[:, :rank], gathered[:, rank:]), step_latent)
    run_max, run_total, run_acc = final
    heads_out = (run_acc / jnp.transpose(run_total)[..., None]).astype(jnp.bfloat16)
    heads_out = heads_out.reshape(tok_rows, local_heads * VDIM)
    return lax.psum_scatter(
        jnp.dot(heads_out, w_out, preferred_element_type=jnp.float32).astype(jnp.bfloat16),
        "tp",
        scatter_dimension=0,
        tiled=True,
    )


def expert_half(tokens_b, ffn_gain, route_expert, route_weight, w_gate, w_up, w_down):
    tok_rows = tokens_b.shape[0]
    expert_count = lax.axis_size("ep")
    capacity = TOPK * tok_rows // expert_count
    normed = rms_scale(tokens_b, ffn_gain)
    copies = route_expert.reshape(tok_rows * TOPK)
    chosen = (copies[:, None] == jnp.arange(expert_count, dtype=jnp.int32)[None, :]).astype(
        jnp.int32
    )
    earlier = jnp.cumsum(chosen, axis=0) - chosen
    slot_index = jnp.sum(earlier * chosen, axis=1)
    target = copies * capacity + slot_index
    source_row = (
        jnp.zeros((expert_count * capacity,), jnp.int32)
        .at[target]
        .set(jnp.arange(tok_rows * TOPK, dtype=jnp.int32) // TOPK)
    )
    outgoing = jnp.take(normed, source_row, axis=0)
    share_cols = outgoing.shape[1] // lax.axis_size("tp")
    own_cols = lax.dynamic_slice_in_dim(outgoing, lax.axis_index("tp") * share_cols, share_cols, 1)
    arrived = lax.all_to_all(own_cols, "ep", split_axis=0, concat_axis=0, tiled=True)
    member = lax.all_gather(arrived, "tp", axis=1, tiled=True)
    gate_rows = w_gate[0]
    up_rows = w_up[0]
    gate_act = jnp.dot(member, gate_rows, preferred_element_type=jnp.float32)
    up_act = jnp.dot(member, up_rows, preferred_element_type=jnp.float32)
    hidden = (jax.nn.silu(gate_act) * up_act).astype(jnp.bfloat16)
    partial_term = jnp.dot(hidden, w_down[0], preferred_element_type=jnp.float32)
    shared = lax.psum_scatter(
        partial_term.astype(jnp.bfloat16), "tp", scatter_dimension=1, tiled=True
    )
    returned = lax.all_to_all(shared, "ep", split_axis=0, concat_axis=0, tiled=True)
    picked = (
        jnp.take(returned, target, axis=0)
        .astype(jnp.float32)
        .reshape(tok_rows, TOPK, returned.shape[1])
    )
    combined = jnp.sum(picked * route_weight[:, :, None], axis=1)
    return combined.astype(jnp.bfloat16)


def flip(index, distance):
    low = index % 2
    high = index // 2
    if distance % 2 == 1:
        low = 1 - low
    if distance // 2 == 1:
        high = 1 - high
    return high * 2 + low


def expert_kernel(
    tokens_ref,
    gain_ref,
    order_ref,
    weight_ref,
    gate_hbm,
    up_hbm,
    down_hbm,
    query_ref,
    latent_ref,
    rope_ref,
    query_gain_ref,
    key_gain_ref,
    cosine_ref,
    sine_ref,
    w_query_ref,
    w_rope_ref,
    w_key_ref,
    w_value_ref,
    w_out_ref,
    fin_ref,
    mixer_ref,
    normed_ref,
    outgoing_ref,
    member_ref,
    gate_ref,
    up_ref,
    down_ref,
    weight_in,
    pair_send,
    pair_keep,
    pair_recv,
    first_send,
    first_keep,
    first_recv,
    second_send,
    second_keep,
    second_recv,
    fin_send,
    keys_ref,
    heads_ref,
    mixed_ref,
    mixed_in,
    joint_send,
    joint_recv,
    load_sem,
    z_send,
    z_recv,
    w_send,
    w_recv,
    x_send,
    x_recv,
    y_send,
    y_recv,
    c_send,
    c_recv,
    p_send,
    p_recv,
    f_send,
    f_recv,
    s_send,
    s_recv,
    o_send,
    o_recv,
    kz_send,
    kz_recv,
    kx_send,
    kx_recv,
    kc_send,
    kc_recv,
    a_send,
    a_recv,
    j_send,
    j_recv,
):
    ep = lax.axis_index("ep")
    tp = lax.axis_index("tp")
    z, x = ep // 2, ep % 2
    y, c = tp // 2, tp % 2
    rows = outgoing_ref.shape[2]
    half = outgoing_ref.shape[3]
    tok_rows = tokens_ref.shape[0]
    share = fin_ref.shape[2]
    spare = rows * SPLIT_NUM // SPLIT_DEN
    carried = pl.ds(pl.multiple_of(y * spare, 16), rows - spare)
    passed = pl.ds(pl.multiple_of(y * (rows - spare), 16), spare)

    def at_z(distance):
        return {"ep": flip(z, distance) * 2 + x, "tp": tp}

    at_x = {"ep": z * 2 + 1 - x, "tp": tp}
    at_y = {"ep": ep, "tp": (1 - y) * 2 + c}
    at_c = {"ep": ep, "tp": y * 2 + 1 - c}

    barrier = pltpu.get_barrier_semaphore()
    for peer in (at_z(1), at_z(2), at_z(3), at_x, at_y, at_c):
        pl.semaphore_signal(barrier, inc=1, device_id=peer, device_id_type=MESH)

    loads = [
        pltpu.make_async_copy(gate_hbm.at[0], gate_ref, load_sem.at[0]),
        pltpu.make_async_copy(up_hbm.at[0], up_ref, load_sem.at[1]),
    ]
    for t in range(4):
        loads.append(
            pltpu.make_async_copy(
                down_hbm.at[0, :, pl.ds(t * share, share)], down_ref.at[t], load_sem.at[2 + t]
            )
        )
    for load in loads:
        load.start()

    def scaled(values_in, gain):
        widened = values_in.astype(jnp.float32)
        mean = jnp.mean(widened * widened, axis=-1, keepdims=True)
        return (widened * lax.rsqrt(mean + epsilon) * gain).astype(jnp.bfloat16)

    turn_shape = (w_rope_ref.shape[1], w_rope_ref.shape[1])
    from_lane = lax.broadcasted_iota(jnp.int32, turn_shape, 0)
    to_lane = lax.broadcasted_iota(jnp.int32, turn_shape, 1)
    to_even = to_lane % 2 == 0
    swap = jnp.where(to_even & (from_lane == to_lane + 1), -1.0, 0.0)
    swap = jnp.where(jnp.logical_not(to_even) & (from_lane == to_lane - 1), 1.0, swap)
    swap = swap.astype(jnp.bfloat16)

    def dot(left, right):
        return jnp.dot(left, right, preferred_element_type=jnp.float32)

    attend_rows, rank = latent_ref.shape
    rope_twice = jnp.concatenate([rope_ref[...]] * 2, axis=1)
    key_turn = rope_twice.astype(jnp.float32) * cosine_ref[...]
    key_turn = key_turn + dot(rope_twice, swap) * sine_ref[...]
    keys_ref[z, x, :, :rank] = scaled(latent_ref[...], key_gain_ref[...])
    keys_ref[z, x, :, rank:] = key_turn.astype(jnp.bfloat16)

    step_rows = 32

    def norm_step(step, unused):
        lines = pl.ds(pl.multiple_of(step * step_rows, step_rows), step_rows)
        normed_ref[lines, :] = scaled(tokens_ref[lines, :], gain_ref[...])
        return unused

    def permuted(group, part):
        lines = pl.ds(pl.multiple_of(group * rows, rows), rows)
        return jnp.dot(
            order_ref[lines, :],
            normed_ref[:, part * half : (part + 1) * half],
            preferred_element_type=jnp.float32,
        ).astype(jnp.bfloat16)

    def remote(source, target, send, recv, peer):
        return pltpu.make_async_remote_copy(
            src_ref=source,
            dst_ref=target,
            send_sem=send,
            recv_sem=recv,
            device_id=peer,
            device_id_type=MESH,
        )

    def z_copy(d):
        return remote(
            outgoing_ref.at[flip(z, d), c, carried],
            member_ref.at[c, z, x, carried],
            z_send.at[d],
            z_recv.at[d],
            at_z(d),
        )

    def w_copy(d):
        return remote(
            weight_ref.at[flip(z, d)], weight_in.at[z], w_send.at[d], w_recv.at[d], at_z(d)
        )

    def x_copy(d):
        block = member_ref.at[c, flip(z, d), x, carried]
        return remote(block, block, x_send.at[d], x_recv.at[d], at_x)

    def y_copy(k):
        line = x if k % 2 == 0 else 1 - x
        block = member_ref.at[c, flip(z, k // 2), line, passed]
        return remote(block, block, y_send.at[k], y_recv.at[k], at_y)

    def c_copy(k):
        line = x if k % 2 == 0 else 1 - x
        block = member_ref.at[c, flip(z, k // 2), line]
        return remote(block, block, c_send.at[k], c_recv.at[k], at_c)

    def p_copy(d):
        return remote(pair_send.at[d], pair_recv.at[d], p_send.at[d], p_recv.at[d], at_c)

    def f_copy(d):
        peer = at_x if d in JOIN_FIRST else at_y
        return remote(first_send.at[d], first_recv.at[d], f_send.at[d], f_recv.at[d], peer)

    def s_copy(d):
        peer = at_y if d in JOIN_FIRST else at_x
        return remote(second_send.at[d], second_recv.at[d], s_send.at[d], s_recv.at[d], peer)

    def o_copy(d):
        return remote(fin_send.at[d], fin_ref.at[z], o_send.at[d], o_recv.at[d], at_z(d))

    key_half = pl.ds(pl.multiple_of(c * (attend_rows // 2), 16), attend_rows // 2)

    def kz_copy(d):
        block = keys_ref.at[z, x, key_half]
        return remote(block, block, kz_send.at[d], kz_recv.at[d], at_z(d))

    def kx_copy(d):
        block = keys_ref.at[flip(z, d), x, key_half]
        return remote(block, block, kx_send.at[d], kx_recv.at[d], at_x)

    def kc_copy(d):
        if d == 0:
            block = keys_ref.at[z, 1 - x, key_half]
        else:
            block = keys_ref.at[flip(z, d), :, key_half]
        return remote(block, block, kc_send.at[d], kc_recv.at[d], at_c)

    def a_copy(yy):
        return remote(
            mixed_ref.at[yy * 2 + 1 - c], mixed_in.at[yy], a_send.at[yy], a_recv.at[yy], at_c
        )

    def j_copy():
        return remote(joint_send, joint_recv, j_send.at[0], j_recv.at[0], at_y)

    started = []

    def start(copy):
        copy.start()
        started.append(copy)

    pl.semaphore_wait(barrier, 6)
    start(kx_copy(0))
    for d in (1, 3, 2):
        start(kz_copy(d))
    lax.fori_loop(0, tok_rows // step_rows, norm_step, 0)
    for part in range(2):
        member_ref[part, z, x] = permuted(z, part)
    start(x_copy(0))
    for d in (1, 3, 2):
        for part in range(2):
            outgoing_ref[flip(z, d), part] = permuted(flip(z, d), part)
        start(z_copy(d))
        start(w_copy(d))

    def compute(d):
        block = flip(z, d)
        low = member_ref[0, block].reshape(2 * rows, half)
        high = member_ref[1, block].reshape(2 * rows, half)

        def project(weights):
            return jnp.dot(
                low, weights[:half, :], preferred_element_type=jnp.float32
            ) + jnp.dot(high, weights[half:, :], preferred_element_type=jnp.float32)

        gate_act = project(gate_ref)
        up_act = project(up_ref)
        hidden = (gate_act / (1.0 + jnp.exp(-gate_act)) * up_act).astype(jnp.bfloat16)
        for yy in range(2):
            term = jnp.dot(hidden, down_ref[yy * 2 + 1 - c], preferred_element_type=jnp.float32)
            pair_send[d, yy] = term.astype(jnp.bfloat16).reshape(2, rows, share)
        start(p_copy(d))
        for yy in range(2):
            term = jnp.dot(hidden, down_ref[yy * 2 + c], preferred_element_type=jnp.float32)
            pair_keep[d, yy] = term.astype(jnp.bfloat16).reshape(2, rows, share)

    def weights_of(d):
        tile = weight_ref[z] if d == 0 else weight_in[flip(z, d)]
        mine = jnp.where(x == 0, tile[0:1], tile[1:2])
        other = jnp.where(x == 0, tile[1:2], tile[0:1])

        def columns(line):
            square = jnp.transpose(jnp.broadcast_to(line, (rows, rows)))
            return jnp.concatenate([square] * (share // rows), axis=1)

        return columns(mine), columns(other)

    def attend():
        query_normed = scaled(query_ref[...], query_gain_ref[...])
        query_nope = dot(query_normed, w_query_ref[...]).astype(jnp.bfloat16)
        swapped = dot(w_rope_ref[...], swap).astype(jnp.bfloat16)
        query_turn = dot(query_normed, w_rope_ref[...]) * cosine_ref[...]
        query_turn = query_turn + dot(query_normed, swapped) * sine_ref[...]
        query_turn = query_turn.astype(jnp.bfloat16)
        count = keys_ref.shape[0] * keys_ref.shape[1] * attend_rows
        keys = keys_ref[...].reshape(count, keys_ref.shape[3])
        latents, turned = keys[:, :rank], keys[:, rank:]
        key_nope = dot(latents, w_key_ref[...]).astype(jnp.bfloat16)
        value_rows = dot(latents, w_value_ref[...]).astype(jnp.bfloat16)
        lane = lax.broadcasted_iota(jnp.int32, query_turn.shape, 1)
        for head in range(w_query_ref.shape[1] // NOPE):
            own = slice(head * NOPE, (head + 1) * NOPE)
            part = jnp.where(lane // ROPE == head, query_turn, jnp.zeros_like(query_turn))
            scores = lax.dot_general(
                jnp.concatenate([query_nope[:, own], part], axis=1),
                jnp.concatenate([key_nope[:, own], turned], axis=1),
                (((1,), (1,)), ((), ())),
                preferred_element_type=jnp.float32,
            )
            scores = scores * (NOPE + ROPE) ** (-0.5)
            raised = jnp.exp(scores - jnp.max(scores, axis=-1, keepdims=True))
            totals = jnp.sum(raised, axis=-1, keepdims=True)
            mixed = dot(raised.astype(jnp.bfloat16), value_rows[:, own]) / totals
            heads_ref[:, own] = mixed.astype(jnp.bfloat16)
        for t in range(4):
            lines = slice(t * (attend_rows // 4), (t + 1) * (attend_rows // 4))
            mixed_ref[t] = dot(heads_ref[lines, :], w_out_ref[...]).astype(jnp.bfloat16)
        for yy in range(2):
            start(a_copy(yy))

    def attend_join():
        for yy in range(2):
            a_copy(yy).wait_recv()
        sums = wide(mixed_ref[(1 - y) * 2 + c]) + wide(mixed_in[1 - y])
        joint_send[...] = sums.astype(jnp.bfloat16)
        start(j_copy())

    def attend_last():
        j_copy().wait_recv()
        sums = wide(mixed_ref[y * 2 + c]) + wide(mixed_in[y]) + wide(joint_recv[...])
        mixer_ref[...] = sums.astype(jnp.bfloat16)

    def wide(value):
        return value.astype(jnp.float32)

    def stage_first(d):
        p_copy(d).wait_recv()
        if d in JOIN_FIRST:
            for yy in range(2):
                sums = wide(pair_keep[d, yy, 1 - x]) + wide(pair_recv[d, yy, 1 - x])
                first_send[d, yy] = sums.astype(jnp.bfloat16)
            start(f_copy(d))
            for yy in range(2):
                first_keep[d, yy] = wide(pair_keep[d, yy, x]) + wide(pair_recv[d, yy, x])
        else:
            for line in range(2):
                sums = wide(pair_keep[d, 1 - y, line]) + wide(pair_recv[d, 1 - y, line])
                first_send[d, line] = sums.astype(jnp.bfloat16)
            start(f_copy(d))
            for line in range(2):
                first_keep[d, line] = wide(pair_keep[d, y, line]) + wide(pair_recv[d, y, line])

    def stage_second(d):
        f_copy(d).wait_recv()
        if d in JOIN_FIRST:
            if d > 0:
                w_copy(d).wait_recv()
            mine, other = weights_of(d)
            sums = mine * first_keep[d, 1 - y] + other * wide(first_recv[d, 1 - y])
            second_send[d] = sums.astype(jnp.bfloat16)
            start(s_copy(d))
            second_keep[d] = mine * first_keep[d, y] + other * wide(first_recv[d, y])
        else:
            sums = first_keep[d, 1 - x] + wide(first_recv[d, 1 - x])
            second_send[d] = sums.astype(jnp.bfloat16)
            start(s_copy(d))
            sums = first_keep[d, x] + wide(first_recv[d, x])
            second_keep[d] = wide(sums.astype(jnp.bfloat16))

    def stage_last(d):
        s_copy(d).wait_recv()
        if d in JOIN_FIRST:
            result = second_keep[d] + wide(second_recv[d])
        else:
            if d > 0:
                w_copy(d).wait_recv()
            mine, other = weights_of(d)
            result = mine * second_keep[d] + other * wide(second_recv[d])
        if d == 0:
            fin_ref[z] = result.astype(jnp.bfloat16)
        else:
            fin_send[d] = result.astype(jnp.bfloat16)
            start(o_copy(d))

    def from_z(d):
        z_copy(d).wait_recv()
        start(x_copy(d))
        start(y_copy(2 * d))

    def from_x(d):
        x_copy(d).wait_recv()
        start(y_copy(2 * d + 1))

    def from_y(k):
        y_copy(k).wait_recv()
        start(c_copy(k))

    for d in (1, 3, 2):
        kz_copy(d).wait_recv()
        start(kx_copy(d))
    for d in (0, 1, 3, 2):
        kx_copy(d).wait_recv()
        start(kc_copy(d))
    from_z(1)
    from_x(0)
    for load in loads:
        load.wait()
    from_y(2)
    from_y(1)
    from_x(1)
    c_copy(1).wait_recv()
    compute(0)
    from_y(3)
    stage_first(0)
    c_copy(2).wait_recv()
    c_copy(3).wait_recv()
    from_z(3)
    compute(1)
    for d in range(4):
        kc_copy(d).wait_recv()
    attend()
    stage_first(1)
    stage_second(0)
    from_z(2)
    from_x(3)
    from_y(6)
    from_x(2)
    from_y(4)
    from_y(7)
    stage_second(1)
    stage_last(0)
    c_copy(6).wait_recv()
    c_copy(7).wait_recv()
    compute(3)
    from_y(5)
    stage_first(3)
    attend_join()
    c_copy(4).wait_recv()
    c_copy(5).wait_recv()
    compute(2)
    stage_last(1)
    stage_first(2)
    stage_second(3)
    attend_last()
    stage_second(2)
    stage_last(3)
    stage_last(2)
    for d in (1, 3, 2):
        o_copy(d).wait_recv()
    for copy in started:
        copy.wait_send()


def expert_exchange(tokens_b, ffn_gain, order, weights, w_gate, w_up, w_down, mixer_args):
    tok_rows, width = tokens_b.shape
    rows = tok_rows // GROUPS
    half = width // 2
    share = width // 4
    units = w_gate.shape[2]
    attend_rows, rank = mixer_args[1].shape
    key_cols = rank + 2 * ROPE
    head_cols = mixer_args[7].shape[1]
    narrow, full = jnp.bfloat16, jnp.float32
    vmem = pl.BlockSpec(memory_space=pltpu.VMEM)
    anywhere = pl.BlockSpec(memory_space=pl.ANY)
    dma = pltpu.SemaphoreType.DMA
    return pl.pallas_call(
        expert_kernel,
        out_shape=(
            jax.ShapeDtypeStruct((GROUPS, rows, share), narrow),
            jax.ShapeDtypeStruct((attend_rows // 4, width), narrow),
        ),
        in_specs=[vmem] * 4 + [anywhere] * 3 + [vmem] * 12,
        out_specs=(vmem, vmem),
        scratch_shapes=[
            pltpu.VMEM((tok_rows, width), narrow),
            pltpu.VMEM((GROUPS, 2, rows, half), narrow),
            pltpu.VMEM((2, GROUPS, 2, rows, half), narrow),
            pltpu.VMEM((width, units), narrow),
            pltpu.VMEM((width, units), narrow),
            pltpu.VMEM((4, units, share), narrow),
            pltpu.VMEM(weights.shape, full),
            pltpu.VMEM((GROUPS, 2, 2, rows, share), narrow),
            pltpu.VMEM((GROUPS, 2, 2, rows, share), narrow),
            pltpu.VMEM((GROUPS, 2, 2, rows, share), narrow),
            pltpu.VMEM((GROUPS, 2, rows, share), narrow),
            pltpu.VMEM((GROUPS, 2, rows, share), full),
            pltpu.VMEM((GROUPS, 2, rows, share), narrow),
            pltpu.VMEM((GROUPS, rows, share), narrow),
            pltpu.VMEM((GROUPS, rows, share), full),
            pltpu.VMEM((GROUPS, rows, share), narrow),
            pltpu.VMEM((GROUPS, rows, share), narrow),
            pltpu.VMEM((GROUPS, 2, attend_rows, key_cols), narrow),
            pltpu.VMEM((attend_rows, head_cols), narrow),
            pltpu.VMEM((4, attend_rows // 4, width), narrow),
            pltpu.VMEM((2, attend_rows // 4, width), narrow),
            pltpu.VMEM((attend_rows // 4, width), narrow),
            pltpu.VMEM((attend_rows // 4, width), narrow),
            dma((6,)),
        ]
        + [dma((4,))] * 6
        + [dma((8,))] * 4
        + [dma((4,))] * 14
        + [dma((2,))] * 4,
        compiler_params=pltpu.CompilerParams(
            collective_id=0, has_side_effects=True, vmem_limit_bytes=52 * 1024 * 1024
        ),
        cost_estimate=pl.CostEstimate(
            flops=40_000_000_000, bytes_accessed=8_000_000, transcendentals=0
        ),
        name="expert_exchange",
    )(tokens_b, ffn_gain.reshape(1, width), order, weights, w_gate, w_up, w_down, *mixer_args)


def lane_tables(tok_rows, width):
    positions = lax.axis_index("ep") * tok_rows + lax.broadcasted_iota(
        jnp.int32, (tok_rows, width), 0
    )
    pair = lax.broadcasted_iota(jnp.int32, (tok_rows, width), 1) % ROPE // 2
    half_width = ROPE // 2
    quarter = half_width // 2
    inverse = rotary_base ** (-(pair % quarter * 2).astype(jnp.float32) / half_width)
    grid_row = (positions // GRID_W).astype(jnp.float32)
    grid_col = (positions % GRID_W).astype(jnp.float32)
    angle = jnp.where(pair < quarter, grid_row, grid_col) * inverse
    return (jnp.cos(angle), jnp.sin(angle))


def paired(mixer, tokens_b, ffn_gain, route_expert, route_weight, w_gate, w_up, w_down):
    tok_rows = tokens_b.shape[0]
    group = route_expert[:, 0] // TOPK
    chosen = (group[:, None] == jnp.arange(GROUPS, dtype=jnp.int32)[None, :]).astype(jnp.bfloat16)
    line = jnp.arange(tok_rows, dtype=jnp.int32)
    before = (line[None, :] < line[:, None]).astype(jnp.bfloat16)
    earlier = jnp.dot(before, chosen, preferred_element_type=jnp.float32)
    rank = jnp.sum(earlier * chosen.astype(jnp.float32), axis=1).astype(jnp.int32)
    place = group * (tok_rows // GROUPS) + rank
    hit = line[:, None] == place[None, :]
    order = hit.astype(jnp.bfloat16)
    first_even = route_expert[:, 0] % TOPK == 0
    even = jnp.where(first_even, route_weight[:, 0], route_weight[:, 1])
    odd = jnp.where(first_even, route_weight[:, 1], route_weight[:, 0])
    sorted_even = jnp.sum(jnp.where(hit, even[None, :], 0.0), axis=1)
    sorted_odd = jnp.sum(jnp.where(hit, odd[None, :], 0.0), axis=1)
    rows = tok_rows // GROUPS
    weights = jnp.stack([sorted_even.reshape(GROUPS, rows), sorted_odd.reshape(GROUPS, rows)], axis=1)
    weights = jnp.pad(weights, ((0, 0), (0, 8 - TOPK), (0, 0)))
    query_latent, key_latent, rope_key, query_gain, key_gain = mixer[:5]
    mixer_args = (
        query_latent,
        key_latent,
        rope_key,
        query_gain.reshape(1, -1),
        key_gain.reshape(1, -1),
        *lane_tables(query_latent.shape[0], 2 * ROPE),
        *mixer[5:],
    )
    fin, mixer_out = expert_exchange(
        tokens_b, ffn_gain, order, weights, w_gate, w_up, w_down, mixer_args
    )
    fin = fin.reshape(tok_rows, fin.shape[2])
    back = lax.dot_general(order, fin, (((0,), (0,)), ((), ())), preferred_element_type=jnp.float32)
    return (mixer_out, back.astype(jnp.bfloat16))


def body(
    query_latent,
    key_latent,
    rope_key,
    query_gain,
    key_gain,
    w_query,
    w_query_rope,
    w_key,
    w_value,
    w_out,
    tokens_b,
    ffn_gain,
    route_expert,
    route_weight,
    w_gate,
    w_up,
    w_down,
):
    mixer = (
        query_latent,
        key_latent,
        rope_key,
        query_gain,
        key_gain,
        w_query,
        w_query_rope,
        w_key,
        w_value,
        w_out,
    )
    experts = (tokens_b, ffn_gain, route_expert, route_weight, w_gate, w_up, w_down)
    if (
        lax.axis_size("ep") == GROUPS * TOPK
        and lax.axis_size("tp") == 4
        and GROUPS == 4
        and tokens_b.shape[0] == GROUPS * 128
        and w_query.shape[1] == 2 * NOPE
    ):
        return paired(mixer, *experts)
    return (mixer_half(*mixer), expert_half(*experts))


def solution(mesh):
    in_specs = (
        P("ep", None),
        P("ep", None),
        P("ep", None),
        P(),
        P(),
        P(None, "tp"),
        P(None, "tp"),
        P(None, "tp"),
        P(None, "tp"),
        P("tp", None),
        P("ep", None),
        P(),
        P("ep", None),
        P("ep", None),
        P("ep", None, "tp"),
        P("ep", None, "tp"),
        P("ep", "tp", None),
    )
    out_specs = (P(("ep", "tp"), None), P("ep", "tp"))
    return jax.shard_map(body, mesh=mesh, in_specs=in_specs, out_specs=out_specs, check_vma=False)
```

profile of v0, /device:TPU:0, one launch (start us, length us, event | category | flops | bytes accessed | tf_op | source)
XLA Modules:
  0.0 90.2 jit_solution(13565013184280229441)
XLA Ops:
  0.7 0.7 fusion.26
  1.4 0.3 fusion
  1.7 0.8 fusion.25
  2.5 0.4 select_reduce_fusion.1
  2.8 0.8 copy.19.rope_ref
  3.7 0.4 fusion.15
  4.0 0.9 %fusion.1.order_ref = bf16[512,512]{1,0:T(8,128)(2,1)} fusion(s32[512]{0:T(512)S(1)} %fusion.20), kind=kLoop, calls=%fused_computation.7 | loop fusion | flops 524288 | bytes 526336 | tf_op jit(solution)/shard_map/convert_element_type | solution.py:739
  5.0 0.0 copy-start
  5.0 0.9 %copy-done = bf16[512,256]{1,0:T(8,128)(2,1)S(1)} copy-done((bf16[512,256]{1,0:T(8,128)(2,1)S(1)}, bf16[512,256]{1,0:T(8,128)(2,1)}, u32[]{:S(2)}) %copy-start) | copy-done | bytes 262168
  5.9 0.0 copy-start.1
  5.9 0.9 %copy-done.1 = bf16[128,512]{1,0:T(8,128)(2,1)S(1)} copy-done((bf16[128,512]{1,0:T(8,128)(2,1)S(1)}, bf16[128,512]{1,0:T(8,128)(2,1)}, u32[]{:S(2)}) %copy-start.1) | copy-done | bytes 131096
  6.8 0.0 copy-start.2
  6.8 0.9 %copy-done.2 = bf16[512,128]{1,0:T(8,128)(2,1)S(1)} copy-done((bf16[512,128]{1,0:T(8,128)(2,1)S(1)}, bf16[512,128]{1,0:T(8,128)(2,1)}, u32[]{:S(2)}) %copy-start.2) | copy-done | bytes 131096
  7.7 0.0 copy-start.3
  7.7 0.9 %copy-done.3 = bf16[256,256]{1,0:T(8,128)(2,1)S(1)} copy-done((bf16[256,256]{1,0:T(8,128)(2,1)S(1)}, bf16[256,256]{1,0:T(8,128)(2,1)}, u32[]{:S(2)}) %copy-start.3) | copy-done | bytes 131096
  8.6 0.0 copy-start.4
  8.6 0.9 %copy-done.4 = bf16[256,256]{1,0:T(8,128)(2,1)S(1)} copy-done((bf16[256,256]{1,0:T(8,128)(2,1)S(1)}, bf16[256,256]{1,0:T(8,128)(2,1)}, u32[]{:S(2)}) %copy-start.4) | copy-done | bytes 131096
  9.5 0.0 copy-start.5
  9.5 0.8 copy-done.5
  10.4 0.0 copy-start.6
  10.4 0.7 copy-done.6
  11.1 0.0 copy-start.7
  11.1 0.7 copy-done.7
  11.8 0.0 copy-start.8
  11.8 0.7 copy-done.8
  12.4 75.8 %expert_exchange.1 = (bf16[4,128,512]{2,1,0:T(8,128)(2,1)S(1)}, bf16[32,2048]{1,0:T(8,128)(2,1)S(1)}) custom-call(bf16[512,2048]{1,0:T(8,128)(2,1)} %tokens_ref.1, f32[1,2048]{1,0:T(1,128)S(1)} %bitcast.11, bf16[512,512]{1,0:T(8,128)(2,1)} %fusion.1.order_ref, f32[4,8,128]{2,1,0:T(8,128)S(1)} %select_maximum_fusion.weight_ref, ...), custom_call_target="tpu_custom_call" | custom-call | flops 40000000000 | bytes 8000000 | tf_op jit(solution)/shard_map/expert_exchange/pallas_call | solution.py:667
  88.3 1.3 %convolution_convert_fusion = bf16[512,512]{1,0:T(8,128)(2,1)} fusion(bf16[512,512]{1,0:T(8,128)(2,1)S(1)} %bitcast.14, s32[512]{0:T(512)S(1)} %fusion.20), kind=kOutput, calls=%fused_computation | convolution fusion | flops 268959744 | bytes 1050624 | tf_op jit(solution)/shard_map/dot_general | solution.py:762
  89.5 0.7 copy.21
  (8 shorter events, 0.1 us)
Async XLA Ops:
  5.0 0.9 %copy-start = (bf16[512,256]{1,0:T(8,128)(2,1)S(1)}, bf16[512,256]{1,0:T(8,128)(2,1)}, u32[]{:S(2)}) copy-start(bf16[512,256]{1,0:T(8,128)(2,1)} %w_query_ref.1) | copy-start | bytes 786436
  5.9 0.9 %copy-start.1 = (bf16[128,512]{1,0:T(8,128)(2,1)S(1)}, bf16[128,512]{1,0:T(8,128)(2,1)}, u32[]{:S(2)}) copy-start(bf16[128,512]{1,0:T(8,128)(2,1)} %query_ref.1) | copy-start | bytes 393220
  6.8 0.9 %copy-start.2 = (bf16[512,128]{1,0:T(8,128)(2,1)S(1)}, bf16[512,128]{1,0:T(8,128)(2,1)}, u32[]{:S(2)}) copy-start(bf16[512,128]{1,0:T(8,128)(2,1)} %w_rope_ref.1) | copy-start | bytes 393220
  7.7 0.9 %copy-start.3 = (bf16[256,256]{1,0:T(8,128)(2,1)S(1)}, bf16[256,256]{1,0:T(8,128)(2,1)}, u32[]{:S(2)}) copy-start(bf16[256,256]{1,0:T(8,128)(2,1)} %w_key_ref.1) | copy-start | bytes 393220
  8.6 0.9 %copy-start.4 = (bf16[256,256]{1,0:T(8,128)(2,1)S(1)}, bf16[256,256]{1,0:T(8,128)(2,1)}, u32[]{:S(2)}) copy-start(bf16[256,256]{1,0:T(8,128)(2,1)} %w_value_ref.1) | copy-start | bytes 393220
  9.5 0.8 copy-start.5
  10.4 0.7 copy-start.6
  11.1 0.7 copy-start.7
  11.8 0.7 copy-start.8
where the time goes:
time: 90.7 us; the launch traced here: 90.2 us
  Pallas kernels  75.8 us (84%)
  local copies, waits for them, and re-layouts  9.71 us (11%)
  other arithmetic  2.43 us (3%)
  matrix products  1.55 us (2%)
    pallas_call x1, Pallas kernels, expert_exchange(): pl.pallas_call(expert_kernel, out_shape=(jax.ShapeDtypeStruct((GROUPS, ro...  75.8 us
    unnamed x20, local copies, waits for them, and re-layouts  8.94 us

commit v1 on v0

v1 whole, which is shorter than its diff:
```python
import functools
import math

import jax
import jax.numpy as jnp
from jax import lax
from jax.experimental import pallas as pl
from jax.experimental.pallas import tpu as pltpu
from jax.sharding import PartitionSpec as P

NOPE = 128
ROPE = 64
VDIM = 128
GRID_W = 64
TOPK = 2
GROUPS = 4
MESH = pl.DeviceIdType.MESH
HALVES = 2
SPARES = (4, 1, 4, 3, 3, 4, 4, 4)
X_LEADS = (0, 2, 3, 5, 7)
SENDS = (2, 0, 1, 6, 3, 7, 4, 5)


epsilon = 1e-06
rotary_base = 10000.0
neg_large = -1e30


def rms_scale(values_in, gain):
    widened = values_in.astype(jnp.float32)
    normed = widened * lax.rsqrt(jnp.mean(widened * widened, axis=-1, keepdims=True) + epsilon)
    return (normed * gain).astype(jnp.bfloat16)


def rotary_tables(positions):
    half_width = ROPE // 2
    inverse = rotary_base ** (-jnp.arange(0, half_width, 2, dtype=jnp.float32) / half_width)
    grid_row = (positions // GRID_W).astype(jnp.float32)
    grid_col = (positions % GRID_W).astype(jnp.float32)
    angle = jnp.concatenate([grid_row[:, None] * inverse, grid_col[:, None] * inverse], axis=-1)
    return (jnp.cos(angle), jnp.sin(angle))


def rotate(values_in, cosine, sine):
    even_part = values_in[..., 0::2]
    odd_part = values_in[..., 1::2]
    turned = jnp.stack(
        [even_part * cosine - odd_part * sine, even_part * sine + odd_part * cosine], axis=-1
    )
    return turned.reshape(values_in.shape)


def fold_blocks(carry, members, step_fn):
    piece_rows = members[0].shape[0]
    block_rows = math.gcd(piece_rows, 1024)
    if block_rows == piece_rows:
        return step_fn(carry, members)
    stacked = tuple(
        (
            member.reshape((piece_rows // block_rows, block_rows) + member.shape[1:])
            for member in members
        )
    )

    def scan_step(inner_carry, blocks):
        return (step_fn(inner_carry, blocks), None)

    result, unused = lax.scan(scan_step, carry, stacked)
    return result


def mixer_half(
    query_latent,
    key_latent,
    rope_key,
    query_gain,
    key_gain,
    w_query,
    w_query_rope,
    w_key,
    w_value,
    w_out,
):
    tok_rows = query_latent.shape[0]
    local_heads = w_query.shape[1] // NOPE
    positions = lax.axis_index("ep") * tok_rows + jnp.arange(tok_rows, dtype=jnp.int32)
    cosine, sine = rotary_tables(positions)
    query_normed = rms_scale(query_latent, query_gain)
    query_nope = jnp.dot(query_normed, w_query, preferred_element_type=jnp.float32).astype(
        jnp.bfloat16
    )
    query_nope = query_nope.reshape(tok_rows, local_heads, NOPE)
    query_rot = jnp.dot(query_normed, w_query_rope, preferred_element_type=jnp.float32)
    query_rot = rotate(
        query_rot.reshape(tok_rows, local_heads, ROPE), cosine[:, None, :], sine[:, None, :]
    )
    query_rot = query_rot.astype(jnp.bfloat16)
    key_rot = rotate(rope_key.astype(jnp.float32), cosine, sine).astype(jnp.bfloat16)
    score_scale = (NOPE + ROPE) ** (-0.5)

    def expand(latent_rows):
        latent_count = latent_rows.shape[0]
        key_normed = rms_scale(latent_rows, key_gain)
        key_nope = jnp.dot(key_normed, w_key, preferred_element_type=jnp.float32).astype(
            jnp.bfloat16
        )
        value_rows = jnp.dot(key_normed, w_value, preferred_element_type=jnp.float32).astype(
            jnp.bfloat16
        )
        return (
            key_nope.reshape(latent_count, local_heads, NOPE),
            value_rows.reshape(latent_count, local_heads, VDIM),
        )

    def attend_block(carry, key_nope, value_rows, key_turn):
        run_max, run_total, run_acc = carry
        scores = jnp.einsum(
            "qhd,khd->hqk", query_nope, key_nope, preferred_element_type=jnp.float32
        )
        scores = scores + jnp.einsum(
            "qhd,kd->hqk", query_rot, key_turn, preferred_element_type=jnp.float32
        )
        scores = scores * score_scale
        new_max = jnp.maximum(run_max, jnp.max(scores, axis=-1))
        correction = jnp.exp(run_max - new_max)
        weights = jnp.exp(scores - new_max[..., None])
        new_total = run_total * correction + jnp.sum(weights, axis=-1)
        added = jnp.einsum(
            "hqk,khd->qhd",
            weights.astype(jnp.bfloat16),
            value_rows,
            preferred_element_type=jnp.float32,
        )
        new_acc = run_acc * jnp.transpose(correction)[..., None] + added
        return (new_max, new_total, new_acc)

    def step_latent(carry, blocks):
        key_nope, value_rows = expand(blocks[0])
        return attend_block(carry, key_nope, value_rows, blocks[1])

    initial = (
        jnp.full((local_heads, tok_rows), neg_large, jnp.float32),
        jnp.zeros((local_heads, tok_rows), jnp.float32),
        jnp.zeros((tok_rows, local_heads, VDIM), jnp.float32),
    )
    gathered = lax.all_gather(
        jnp.concatenate([key_latent, key_rot], axis=1), "ep", axis=0, tiled=True
    )
    rank = key_latent.shape[1]
    final = fold_blocks(initial, (gathered[:, :rank], gathered[:, rank:]), step_latent)
    run_max, run_total, run_acc = final
    heads_out = (run_acc / jnp.transpose(run_total)[..., None]).astype(jnp.bfloat16)
    heads_out = heads_out.reshape(tok_rows, local_heads * VDIM)
    return lax.psum_scatter(
        jnp.dot(heads_out, w_out, preferred_element_type=jnp.float32).astype(jnp.bfloat16),
        "tp",
        scatter_dimension=0,
        tiled=True,
    )


def expert_half(tokens_b, ffn_gain, route_expert, route_weight, w_gate, w_up, w_down):
    tok_rows = tokens_b.shape[0]
    expert_count = lax.axis_size("ep")
    capacity = TOPK * tok_rows // expert_count
    normed = rms_scale(tokens_b, ffn_gain)
    copies = route_expert.reshape(tok_rows * TOPK)
    chosen = (copies[:, None] == jnp.arange(expert_count, dtype=jnp.int32)[None, :]).astype(
        jnp.int32
    )
    earlier = jnp.cumsum(chosen, axis=0) - chosen
    slot_index = jnp.sum(earlier * chosen, axis=1)
    target = copies * capacity + slot_index
    source_row = (
        jnp.zeros((expert_count * capacity,), jnp.int32)
        .at[target]
        .set(jnp.arange(tok_rows * TOPK, dtype=jnp.int32) // TOPK)
    )
    outgoing = jnp.take(normed, source_row, axis=0)
    share_cols = outgoing.shape[1] // lax.axis_size("tp")
    own_cols = lax.dynamic_slice_in_dim(outgoing, lax.axis_index("tp") * share_cols, share_cols, 1)
    arrived = lax.all_to_all(own_cols, "ep", split_axis=0, concat_axis=0, tiled=True)
    member = lax.all_gather(arrived, "tp", axis=1, tiled=True)
    gate_rows = w_gate[0]
    up_rows = w_up[0]
    gate_act = jnp.dot(member, gate_rows, preferred_element_type=jnp.float32)
    up_act = jnp.dot(member, up_rows, preferred_element_type=jnp.float32)
    hidden = (jax.nn.silu(gate_act) * up_act).astype(jnp.bfloat16)
    partial_term = jnp.dot(hidden, w_down[0], preferred_element_type=jnp.float32)
    shared = lax.psum_scatter(
        partial_term.astype(jnp.bfloat16), "tp", scatter_dimension=1, tiled=True
    )
    returned = lax.all_to_all(shared, "ep", split_axis=0, concat_axis=0, tiled=True)
    picked = (
        jnp.take(returned, target, axis=0)
        .astype(jnp.float32)
        .reshape(tok_rows, TOPK, returned.shape[1])
    )
    combined = jnp.sum(picked * route_weight[:, :, None], axis=1)
    return combined.astype(jnp.bfloat16)


def flip(index, distance):
    low = index % 2
    high = index // 2
    if distance % 2 == 1:
        low = 1 - low
    if distance // 2 == 1:
        high = 1 - high
    return high * 2 + low


def expert_kernel(
    tokens_hbm,
    gain_hbm,
    route_hbm,
    weight_hbm,
    gate_hbm,
    up_hbm,
    down_hbm,
    query_hbm,
    latent_hbm,
    rope_hbm,
    query_gain_hbm,
    key_gain_hbm,
    w_query_hbm,
    w_rope_hbm,
    w_key_hbm,
    w_value_hbm,
    w_out_hbm,
    moe_ref,
    mixer_ref,
    tokens_ref,
    gain_ref,
    route_ref,
    share_ref,
    query_ref,
    latent_ref,
    rope_ref,
    query_gain_ref,
    key_gain_ref,
    w_query_ref,
    w_rope_ref,
    w_key_ref,
    w_value_ref,
    w_out_ref,
    order_ref,
    back_ref,
    weight_ref,
    weight_in,
    column_ref,
    scale_ref,
    outgoing_ref,
    member_ref,
    gate_ref,
    up_ref,
    down_ref,
    pair_send,
    pair_keep,
    pair_recv,
    first_send,
    first_keep,
    first_recv,
    second_send,
    second_keep,
    second_recv,
    fin_send,
    fin_ref,
    keys_ref,
    turns_ref,
    query_nope_ref,
    query_turn_ref,
    heads_ref,
    mixed_ref,
    mixed_in,
    joint_send,
    joint_recv,
    token_sem,
    load_sem,
    z_send,
    z_recv,
    x_send,
    x_recv,
    y_send,
    y_recv,
    c_send,
    c_recv,
    p_send,
    p_recv,
    f_send,
    f_recv,
    s_send,
    s_recv,
    o_send,
    o_recv,
    w_send,
    w_recv,
    kz_send,
    kz_recv,
    kx_send,
    kx_recv,
    kc_send,
    kc_recv,
    a_send,
    a_recv,
    j_send,
    j_recv,
):
    ep = lax.axis_index("ep")
    tp = lax.axis_index("tp")
    z, x = ep // 2, ep % 2
    y, c = tp // 2, tp % 2
    rows, half = outgoing_ref.shape[1:]
    lines_of = rows // HALVES
    tok_rows = tokens_ref.shape[0]
    share = fin_ref.shape[2]

    def spare_of(u):
        return half * SPARES[u] // 8

    def carried(u):
        return pl.ds(pl.multiple_of(y * spare_of(u), 128), half - spare_of(u))

    def passed(u):
        return pl.ds(pl.multiple_of(y * (half - spare_of(u)), 128), spare_of(u))

    at_end = (z == 0) | (z == GROUPS - 1)

    def at_z(distance):
        return {"ep": flip(z, distance) * 2 + x, "tp": tp}

    at_x = {"ep": z * 2 + 1 - x, "tp": tp}
    at_y = {"ep": ep, "tp": (1 - y) * 2 + c}
    at_c = {"ep": ep, "tp": y * 2 + 1 - c}

    barrier = pltpu.get_barrier_semaphore()
    for peer in (at_z(1), at_z(2), at_z(3), at_x, at_y, at_c):
        pl.semaphore_signal(barrier, inc=1, device_id=peer, device_id_type=MESH)

    loads = {}

    def load(name, source, target):
        loads[name] = pltpu.make_async_copy(source, target, load_sem.at[len(loads)])
        loads[name].start()

    load("route", route_hbm, route_ref)
    load("gain", gain_hbm, gain_ref)
    token_loads = []
    for k in range(4):
        lines = pl.ds(k * (tok_rows // 4), tok_rows // 4)
        token_loads.append(
            pltpu.make_async_copy(tokens_hbm.at[lines], tokens_ref.at[lines], token_sem.at[k])
        )
        token_loads[k].start()
    load("share", weight_hbm, share_ref)
    load("key_gain", key_gain_hbm, key_gain_ref)
    load("latent", latent_hbm, latent_ref)
    load("rope", rope_hbm, rope_ref)
    load("gate", gate_hbm.at[0], gate_ref)
    load("up", up_hbm.at[0], up_ref)
    for t in range(4):
        load(("down", t), down_hbm.at[0, :, pl.ds(t * share, share)], down_ref.at[t])
    load("query_gain", query_gain_hbm, query_gain_ref)
    load("query", query_hbm, query_ref)
    load("w_query", w_query_hbm, w_query_ref)
    load("w_rope", w_rope_hbm, w_rope_ref)
    load("w_key", w_key_hbm, w_key_ref)
    load("w_value", w_value_hbm, w_value_ref)
    load("w_out", w_out_hbm, w_out_ref)

    def dot(left, right):
        return jnp.dot(left, right, preferred_element_type=jnp.float32)

    def dot_lanes(left, right):
        return lax.dot_general(
            left, right, (((1,), (1,)), ((), ())), preferred_element_type=jnp.float32
        )

    def wide(value):
        return value.astype(jnp.float32)

    def scaled(values_in, gain):
        widened = wide(values_in)
        mean = jnp.mean(widened * widened, axis=-1, keepdims=True)
        return (widened * lax.rsqrt(mean + epsilon) * gain).astype(jnp.bfloat16)

    def iota(shape, dim):
        return lax.broadcasted_iota(jnp.int32, shape, dim)

    def group_lines(group):
        return pl.ds(pl.multiple_of(group * rows, rows), rows)

    before = jnp.where(iota((tok_rows, tok_rows), 0) < iota((tok_rows, tok_rows), 1), 1.0, 0.0)
    before = before.astype(jnp.bfloat16)
    loads["route"].wait()
    first = route_ref[0:1, :]
    group = jnp.zeros_like(first)
    for g in range(1, GROUPS):
        group = group + (first >= g * TOPK).astype(jnp.int32)
    picks = jnp.broadcast_to(group, (8, tok_rows)) == iota((8, tok_rows), 0)
    picks = jnp.where(picks, 1.0, 0.0)
    earlier = dot(picks.astype(jnp.bfloat16), before)
    rank_of = jnp.sum(earlier * picks, axis=0, keepdims=True).astype(jnp.int32)
    place = group * rows + rank_of
    for g in range(GROUPS):
        hit = jnp.broadcast_to(place, (rows, tok_rows)) == iota((rows, tok_rows), 0) + g * rows
        order_ref[g * rows : (g + 1) * rows, :] = jnp.where(hit, 1.0, 0.0).astype(jnp.bfloat16)

    def split(value):
        top = value.astype(jnp.bfloat16)
        rest = value - wide(top)
        middle = rest.astype(jnp.bfloat16)
        return wide(top), wide(middle), rest - wide(middle)

    step_rows = 32

    def scale_step(step, unused):
        lines = pl.ds(pl.multiple_of(step * step_rows, step_rows), step_rows)
        widened = wide(tokens_ref[lines, :])
        mean = jnp.mean(widened * widened, axis=-1, keepdims=True)
        lane = iota((step_rows, 128), 1)
        table = jnp.zeros((step_rows, 128), jnp.float32)
        for k, value in enumerate(split(lax.rsqrt(mean + epsilon))):
            table = jnp.where(lane == k, jnp.broadcast_to(value, table.shape), table)
        scale_ref[lines, :] = table.astype(jnp.bfloat16)
        return unused

    per_load = tok_rows // 4 // step_rows
    for k in range(4):
        token_loads[k].wait()
        lax.fori_loop(k * per_load, (k + 1) * per_load, scale_step, 0, unroll=True)
    loads["gain"].wait()

    def remote(source, target, send, recv, peer):
        return pltpu.make_async_remote_copy(
            src_ref=source,
            dst_ref=target,
            send_sem=send,
            recv_sem=recv,
            device_id=peer,
            device_id_type=MESH,
        )

    def lines_at(u):
        return pl.ds(u % HALVES * lines_of, lines_of)

    def block_at(u):
        return flip(z, u // HALVES)

    def line_at(rel):
        return x if rel == 0 else 1 - x

    def z_copy(u):
        return remote(
            outgoing_ref.at[block_at(u), lines_at(u), carried(u)],
            member_ref.at[c, z, x, lines_at(u), carried(u)],
            z_send.at[u],
            z_recv.at[u],
            at_z(u // HALVES),
        )

    def w_copy(d):
        return remote(
            weight_ref.at[flip(z, d)], weight_in.at[z], w_send.at[d], w_recv.at[d], at_z(d)
        )

    def x_copy(u):
        piece = member_ref.at[c, block_at(u), x, lines_at(u), carried(u)]
        return remote(piece, piece, x_send.at[u], x_recv.at[u], at_x)

    def y_copy(u, rel):
        piece = member_ref.at[c, block_at(u), line_at(rel), lines_at(u), passed(u)]
        k = 2 * u + rel
        return remote(piece, piece, y_send.at[k], y_recv.at[k], at_y)

    def c_copy(u, rel):
        piece = member_ref.at[c, block_at(u), line_at(rel), lines_at(u)]
        k = 2 * u + rel
        return remote(piece, piece, c_send.at[k], c_recv.at[k], at_c)

    def p_copy(u):
        return remote(pair_send.at[u], pair_recv.at[u], p_send.at[u], p_recv.at[u], at_c)

    def x_leads(u):
        return u in X_LEADS

    def f_copy(u):
        peer = at_x if x_leads(u) else at_y
        return remote(first_send.at[u], first_recv.at[u], f_send.at[u], f_recv.at[u], peer)

    def s_copy(u):
        peer = at_y if x_leads(u) else at_x
        return remote(second_send.at[u], second_recv.at[u], s_send.at[u], s_recv.at[u], peer)

    def o_copy(u):
        return remote(
            fin_send.at[u],
            fin_ref.at[z, lines_at(u)],
            o_send.at[u],
            o_recv.at[u],
            at_z(u // HALVES),
        )

    def key_pair(view, send, recv, k, peer):
        return [
            remote(ref, ref, send.at[2 * k + i], recv.at[2 * k + i], peer)
            for i, ref in enumerate(view)
        ]

    def kz_copy(d):
        view = (keys_ref.at[z, x, c], turns_ref.at[z, x, c])
        return key_pair(view, kz_send, kz_recv, d, at_z(d))

    def kx_copy(d):
        view = (keys_ref.at[flip(z, d), x, c], turns_ref.at[flip(z, d), x, c])
        return key_pair(view, kx_send, kx_recv, d, at_x)

    def kc_copy(d):
        if d == 0:
            view = (keys_ref.at[z, 1 - x, c], turns_ref.at[z, 1 - x, c])
        else:
            view = (keys_ref.at[flip(z, d), :, c], turns_ref.at[flip(z, d), :, c])
        return key_pair(view, kc_send, kc_recv, d, at_c)

    def a_copy(yy):
        return remote(
            mixed_ref.at[yy * 2 + 1 - c], mixed_in.at[yy], a_send.at[yy], a_recv.at[yy], at_c
        )

    def j_copy():
        return remote(joint_send, joint_recv, j_send.at[0], j_recv.at[0], at_y)

    started = []

    def copies_of(maker, args):
        made = maker(*args)
        return made if isinstance(made, list) else [made]

    def start(maker, *args):
        for copy in copies_of(maker, args):
            copy.start()
        if (maker, args) not in started:
            started.append((maker, args))

    def arrive(maker, *args):
        for copy in copies_of(maker, args):
            copy.wait_recv()

    def scale_of(group_index):
        table = dot(order_ref[group_lines(group_index), :], scale_ref[...])
        return jnp.sum(table, axis=-1, keepdims=True)

    def permuted(group_index, scale, first_col, cols):
        place_of = pl.ds(pl.multiple_of(first_col, 128), cols)
        picked = dot(order_ref[group_lines(group_index), :], tokens_ref[:, place_of])
        return (picked * scale * gain_ref[:, place_of]).astype(jnp.bfloat16)

    def make_units(d):
        spare = min(spare_of(d * HALVES + h) for h in range(HALVES))
        kept = pl.ds(pl.multiple_of(y * spare, 128), half - spare)
        outgoing_ref[flip(z, d), :, kept] = permuted(
            flip(z, d), scale_of(flip(z, d)), c * half + y * spare, half - spare
        )

    def make_own():
        scale = scale_of(z)
        for part in range(2):
            member_ref[part, z, x] = permuted(z, scale, part * half, half)

    made = set()
    for u in SENDS:
        d = u // HALVES
        if d not in made:
            if d > 0:
                make_units(d)
            else:
                make_own()
            if not made:
                pl.semaphore_wait(barrier, 6)
            made.add(d)
        if d > 0:
            start(z_copy, u)
        else:
            start(x_copy, u)

    def send_weights():
        loads["share"].wait()
        first_is_even = picks_even(route_ref[0:1, :])
        even = jnp.where(first_is_even, share_ref[0:1, :], share_ref[1:2, :])
        odd = jnp.where(first_is_even, share_ref[1:2, :], share_ref[0:1, :])
        line = iota((8, tok_rows), 0)
        table = jnp.zeros((8, tok_rows), jnp.float32)
        for k, value in enumerate(split(even) + split(odd)):
            table = jnp.where(line == k, jnp.broadcast_to(value, table.shape), table)
        table = table.astype(jnp.bfloat16)
        for g in range(GROUPS):
            weight_ref[g] = dot_lanes(table, order_ref[g * rows : (g + 1) * rows, :])
        for d in (1, 3, 2):
            start(w_copy, d)

    def picks_even(chosen):
        odd = jnp.zeros(chosen.shape, jnp.bool_)
        for e in range(1, GROUPS * TOPK, TOPK):
            odd = odd | (chosen == e)
        return jnp.logical_not(odd)

    def set_columns(d):
        if d > 0:
            arrive(w_copy, d)
        tile = weight_ref[z] if d == 0 else weight_in[flip(z, d)]
        even = tile[0:1] + tile[1:2] + tile[2:3]
        odd = tile[3:4] + tile[4:5] + tile[5:6]
        for k, line in enumerate(
            (jnp.where(x == 0, even, odd), jnp.where(x == 0, odd, even))
        ):
            column_ref[d, k] = jnp.transpose(jnp.broadcast_to(line, (rows, rows)))

    attend_rows, rank = latent_ref.shape
    key_half = attend_rows // 2
    lanes = 2 * ROPE

    def tables():
        lane = iota((1, lanes), 1)
        pair = (lane & (ROPE - 1)) >> 1
        quarter = ROPE // 4
        inverse = jnp.zeros((1, lanes), jnp.float32)
        for j in range(quarter):
            rate = rotary_base ** (-2.0 * j / (ROPE // 2))
            inverse = jnp.where((pair & (quarter - 1)) == j, rate, inverse)
        position = (ep * attend_rows + iota((attend_rows, lanes), 0)).astype(jnp.float32)
        grid_row = jnp.floor(position * (1.0 / GRID_W))
        grid_col = position - grid_row * GRID_W
        angle = jnp.where(jnp.broadcast_to(pair, position.shape) < quarter, grid_row, grid_col)
        angle = angle * inverse
        return jnp.cos(angle), jnp.sin(angle)

    def swap_matrix():
        from_lane = iota((lanes, lanes), 0)
        to_lane = iota((lanes, lanes), 1)
        to_even = (to_lane & 1) == 0
        swap = jnp.where(to_even & (from_lane == to_lane + 1), -1.0, 0.0)
        swap = jnp.where(jnp.logical_not(to_even) & (from_lane == to_lane - 1), 1.0, swap)
        return swap.astype(jnp.bfloat16)

    def make_keys():
        cosine, sine = tables()
        swap = swap_matrix()
        low_lane = iota((key_half, lanes), 1) < ROPE
        for name in ("key_gain", "latent", "rope"):
            loads[name].wait()
        keys_ref[z, x] = scaled(latent_ref[...], key_gain_ref[...]).reshape(2, key_half, rank)
        twice = jnp.transpose(jnp.concatenate([wide(rope_ref[...])] * 2, axis=0))
        turned = twice * cosine + dot(twice.astype(jnp.bfloat16), swap) * sine
        packed = jnp.where(low_lane, turned[:key_half], turned[key_half:])
        turns_ref[z, x] = packed.astype(jnp.bfloat16).reshape(2, key_half // 2, lanes)
        start(kx_copy, 0)
        for d in (1, 3, 2):
            start(kz_copy, d)
        for name in ("query_gain", "query", "w_query", "w_rope"):
            loads[name].wait()
        query_normed = scaled(query_ref[...], query_gain_ref[...])
        query_nope_ref[...] = dot(query_normed, w_query_ref[...]).astype(jnp.bfloat16)
        swapped = dot(w_rope_ref[...], swap).astype(jnp.bfloat16)
        query_turn = dot(query_normed, w_rope_ref[...]) * cosine
        query_turn = query_turn + dot(query_normed, swapped) * sine
        low = iota((attend_rows, lanes), 1) < ROPE
        for head in range(2):
            own = jnp.where(low if head == 0 else jnp.logical_not(low), query_turn, 0.0)
            other = pltpu.roll(own, ROPE, 1)
            query_turn_ref[head, head] = own.astype(jnp.bfloat16)
            query_turn_ref[head, 1 - head] = other.astype(jnp.bfloat16)

    def make_back():
        for k in range(tok_rows // rows):
            spread = jnp.broadcast_to(wide(place[:, k * rows : (k + 1) * rows]), (rows, rows))
            spread = jnp.transpose(spread)
            for g in range(GROUPS):
                target = (iota((rows, rows), 1) + g * rows).astype(jnp.float32)
                hit = jnp.where(spread == target, 1.0, 0.0).astype(jnp.bfloat16)
                back_ref[g, k * rows : (k + 1) * rows, :] = hit

    def compute(u):
        low = member_ref[0, block_at(u), :, lines_at(u), :].reshape(2 * lines_of, half)
        high = member_ref[1, block_at(u), :, lines_at(u), :].reshape(2 * lines_of, half)

        def project(weights):
            return dot(low, weights[:half, :]) + dot(high, weights[half:, :])

        gate_act = project(gate_ref)
        up_act = project(up_ref)
        hidden = (gate_act / (1.0 + jnp.exp(-gate_act)) * up_act).astype(jnp.bfloat16)
        for yy in range(2):
            term = dot(hidden, down_ref[yy * 2 + 1 - c])
            pair_send[u, yy] = term.astype(jnp.bfloat16).reshape(2, lines_of, share)
        start(p_copy, u)
        for yy in range(2):
            term = dot(hidden, down_ref[yy * 2 + c])
            pair_keep[u, yy] = term.astype(jnp.bfloat16).reshape(2, lines_of, share)

    def weights_of(u):
        def columns(k):
            square = column_ref[u // HALVES, k, lines_at(u), :]
            return jnp.concatenate([square] * (share // rows), axis=1)

        return columns(0), columns(1)

    def attend():
        for name in ("w_key", "w_value", "w_out"):
            loads[name].wait()
        blocks = keys_ref.shape[0] * keys_ref.shape[1]
        latents = keys_ref[...].reshape(blocks * attend_rows, rank)
        turns = turns_ref[...].reshape(blocks * key_half, lanes)
        key_nope = dot(latents, w_key_ref[...]).astype(jnp.bfloat16)
        value_rows = dot(latents, w_value_ref[...]).astype(jnp.bfloat16)
        key_nope = key_nope.reshape(blocks, 2, key_half, key_nope.shape[1])
        value_rows = value_rows.reshape(blocks, 2, key_half, value_rows.shape[1])
        for head in range(w_query_ref.shape[1] // NOPE):
            own = slice(head * NOPE, (head + 1) * NOPE)
            scores = []
            for part in range(2):
                left = jnp.concatenate(
                    [query_nope_ref[:, own], query_turn_ref[head, part]], axis=1
                )
                keys = key_nope[:, part, :, own].reshape(blocks * key_half, NOPE)
                right = jnp.concatenate([keys, turns], axis=1)
                scores.append(dot_lanes(left, right) * (NOPE + ROPE) ** (-0.5))
            top = jnp.maximum(
                jnp.max(scores[0], axis=-1, keepdims=True),
                jnp.max(scores[1], axis=-1, keepdims=True),
            )
            totals = jnp.zeros(top.shape, jnp.float32)
            mixed = jnp.zeros((attend_rows, VDIM), jnp.float32)
            for part in range(2):
                raised = jnp.exp(scores[part] - top)
                totals = totals + jnp.sum(raised, axis=-1, keepdims=True)
                values = value_rows[:, part, :, own].reshape(blocks * key_half, VDIM)
                mixed = mixed + dot(raised.astype(jnp.bfloat16), values)
            heads_ref[:, own] = (mixed / totals).astype(jnp.bfloat16)
        for t in range(4):
            lines = slice(t * (attend_rows // 4), (t + 1) * (attend_rows // 4))
            mixed_ref[t] = dot(heads_ref[lines, :], w_out_ref[...]).astype(jnp.bfloat16)
        for yy in range(2):
            start(a_copy, yy)

    def attend_join():
        for yy in range(2):
            arrive(a_copy, yy)
        sums = wide(mixed_ref[(1 - y) * 2 + c]) + wide(mixed_in[1 - y])
        joint_send[...] = sums.astype(jnp.bfloat16)
        start(j_copy)

    def attend_last():
        arrive(j_copy)
        sums = wide(mixed_ref[y * 2 + c]) + wide(mixed_in[y]) + wide(joint_recv[...])
        mixer_ref[...] = sums.astype(jnp.bfloat16)

    def stage_first(u):
        arrive(p_copy, u)
        if x_leads(u):
            for yy in range(2):
                sums = wide(pair_keep[u, yy, 1 - x]) + wide(pair_recv[u, yy, 1 - x])
                first_send[u, yy] = sums.astype(jnp.bfloat16)
            start(f_copy, u)
            for yy in range(2):
                first_keep[u, yy] = wide(pair_keep[u, yy, x]) + wide(pair_recv[u, yy, x])
        else:
            for line in range(2):
                sums = wide(pair_keep[u, 1 - y, line]) + wide(pair_recv[u, 1 - y, line])
                first_send[u, line] = sums.astype(jnp.bfloat16)
            start(f_copy, u)
            for line in range(2):
                first_keep[u, line] = wide(pair_keep[u, y, line]) + wide(pair_recv[u, y, line])

    def stage_second(u):
        arrive(f_copy, u)
        if x_leads(u):
            mine, other = weights_of(u)
            sums = mine * first_keep[u, 1 - y] + other * wide(first_recv[u, 1 - y])
            second_send[u] = sums.astype(jnp.bfloat16)
            start(s_copy, u)
            second_keep[u] = mine * first_keep[u, y] + other * wide(first_recv[u, y])
        else:
            sums = first_keep[u, 1 - x] + wide(first_recv[u, 1 - x])
            second_send[u] = sums.astype(jnp.bfloat16)
            start(s_copy, u)
            sums = first_keep[u, x] + wide(first_recv[u, x])
            second_keep[u] = wide(sums.astype(jnp.bfloat16))

    def stage_last(u):
        arrive(s_copy, u)
        if x_leads(u):
            result = second_keep[u] + wide(second_recv[u])
        else:
            mine, other = weights_of(u)
            result = mine * second_keep[u] + other * wide(second_recv[u])
        if u // HALVES == 0:
            fin_ref[z, lines_at(u)] = result.astype(jnp.bfloat16)
        else:
            fin_send[u] = result.astype(jnp.bfloat16)
            start(o_copy, u)

    def from_z(u):
        arrive(z_copy, u)
        start(x_copy, u)
        start(y_copy, u, 0)

    def from_x(u):
        arrive(x_copy, u)
        start(y_copy, u, 1)

    def from_y(u, rel):
        arrive(y_copy, u, rel)
        start(c_copy, u, rel)

    def gathered(u):
        for rel in range(2):
            if u // HALVES > 0 or rel > 0:
                arrive(c_copy, u, rel)

    def wait_weights():
        for name in ("gate", "up"):
            loads[name].wait()
        for t in range(4):
            loads[("down", t)].wait()

    def from_kz(d):
        arrive(kz_copy, d)
        start(kx_copy, d)

    def from_kx(d):
        arrive(kx_copy, d)
        start(kc_copy, d)

    def from_kc(d):
        arrive(kc_copy, d)

    def back_term(d):
        return dot(back_ref[flip(z, d)], fin_ref[flip(z, d)])

    def returned(u):
        arrive(o_copy, u)

    def back_early():
        for d in (1, 3):
            for h in range(HALVES):
                returned(d * HALVES + h)
        moe_ref[...] = (back_term(0) + back_term(1) + back_term(3)).astype(jnp.bfloat16)

    def back_last():
        for h in range(HALVES):
            returned(2 * HALVES + h)
        moe_ref[...] = (wide(moe_ref[...]) + back_term(2)).astype(jnp.bfloat16)

    steps = {
        "z": from_z,
        "x": from_x,
        "y": from_y,
        "g": gathered,
        "m": compute,
        "1": stage_first,
        "2": stage_second,
        "3": stage_last,
        "weights": send_weights,
        "columns": set_columns,
        "keys": make_keys,
        "back": make_back,
        "loaded": wait_weights,
        "kz": from_kz,
        "kx": from_kx,
        "kc": from_kc,
        "attend": attend,
        "join": attend_join,
        "last": attend_last,
        "early": back_early,
        "final": back_last,
    }

    for item in SCHEDULE:
            where, text = "", item
            if item[0] in "<>":
                where, text = item[0], item[1:]
            name, *numbers = text.split(".")
            step = steps[name]
            values = [int(number) for number in numbers]
            if where == "":
                step(*values)
            else:
                pl.when(at_end if where == ">" else jnp.logical_not(at_end))(
                    functools.partial(step, *values)
                )
    for maker, args in started:
        for copy in copies_of(maker, args):
            copy.wait_send()


SCHEDULE = (
    "keys", "loaded", "<x.1", "z.2", "back", "x.0", "z.3", ">y.0.1", ">x.1", ">z.6", ">kz.1", "x.2",
    ">y.2.0", ">x.3", ">y.6.0", "z.7", "kx.0", ">y.1.1", "<z.6", "<y.2.0", "<y.0.1", "g.0", "m.0",
    ">kc.0", ">z.5", ">kx.1", "<x.3", "<y.1.1", "weights", "<kz.3", "<y.2.1", "<z.4", "<x.6",
    "<y.3.1", "<z.5", "<x.7", "<y.6.0", "<kz.1", "<y.3.0", "<y.4.0", "<y.6.1", "1.0", ">z.4", "g.1",
    "m.1", ">x.6", ">y.2.1", "<kz.2", "<x.5", "y.7.0", ">x.7", "g.2", "m.2", ">kz.2", ">y.3.0",
    ">x.5", ">y.5.0", ">y.3.1", "columns.2", "columns.1", ">y.6.1", ">y.4.0", ">kz.3", "<kc.0",
    "<kx.1", "<y.5.0", "<y.7.1", "1.1", "columns.0", "<x.4", "1.2", "g.3", "m.3", "g.6", "m.6",
    ">y.5.1", ">x.4", "1.3", "<kx.2", "<kc.1", "<kx.3", "<y.5.1", "1.6", ">y.7.1", ">kx.3", ">kx.2",
    ">kc.1", ">kc.2", "g.5", "m.5", ">y.4.1", "2.1", "2.2", "<kc.3", "<y.4.1", "g.7", "m.7", "1.5",
    "2.0", "2.3", "g.4", "m.4", ">kc.3", "2.6", "<kc.2", "3.1", "1.4", "columns.3", "1.7", "3.2",
    "attend", "2.5", "3.0", "3.6", "3.3", "join", "2.4", "2.7", "3.5", "3.4", "3.7", "last",
    "early", "final",
)


def expert_exchange(tokens_b, ffn_gain, route, share_of, w_gate, w_up, w_down, mixer_args):
    tok_rows, width = tokens_b.shape
    rows = tok_rows // GROUPS
    half = width // 2
    share = width // 4
    units = w_gate.shape[2]
    attend_rows, rank = mixer_args[1].shape
    head_cols = mixer_args[7].shape[1]
    rank_q = mixer_args[0].shape[1]
    count = GROUPS * HALVES
    part = rows // HALVES
    narrow, full = jnp.bfloat16, jnp.float32
    vmem = pl.BlockSpec(memory_space=pltpu.VMEM)
    anywhere = pl.BlockSpec(memory_space=pl.ANY)
    dma = pltpu.SemaphoreType.DMA
    operands = (
        tokens_b,
        ffn_gain.reshape(1, width),
        route,
        share_of,
        w_gate,
        w_up,
        w_down,
        *mixer_args,
    )
    return pl.pallas_call(
        expert_kernel,
        out_shape=(
            jax.ShapeDtypeStruct((tok_rows, share), narrow),
            jax.ShapeDtypeStruct((attend_rows // 4, width), narrow),
        ),
        in_specs=[anywhere] * len(operands),
        out_specs=(vmem, vmem),
        scratch_shapes=[
            pltpu.VMEM((tok_rows, width), narrow),
            pltpu.VMEM((1, width), full),
            pltpu.VMEM(route.shape, jnp.int32),
            pltpu.VMEM(share_of.shape, full),
            pltpu.VMEM((attend_rows, rank_q), narrow),
            pltpu.VMEM((attend_rows, rank), narrow),
            pltpu.VMEM((ROPE, attend_rows), narrow),
            pltpu.VMEM((1, rank_q), full),
            pltpu.VMEM((1, rank), full),
            pltpu.VMEM(mixer_args[5].shape, narrow),
            pltpu.VMEM(mixer_args[6].shape, narrow),
            pltpu.VMEM(mixer_args[7].shape, narrow),
            pltpu.VMEM(mixer_args[8].shape, narrow),
            pltpu.VMEM(mixer_args[9].shape, narrow),
            pltpu.VMEM((tok_rows, tok_rows), narrow),
            pltpu.VMEM((GROUPS, tok_rows, rows), narrow),
            pltpu.VMEM((GROUPS, 8, rows), full),
            pltpu.VMEM((GROUPS, 8, rows), full),
            pltpu.VMEM((GROUPS, 2, rows, rows), full),
            pltpu.VMEM((tok_rows, 128), narrow),
            pltpu.VMEM((GROUPS, rows, half), narrow),
            pltpu.VMEM((2, GROUPS, 2, rows, half), narrow),
            pltpu.VMEM((width, units), narrow),
            pltpu.VMEM((width, units), narrow),
            pltpu.VMEM((4, units, share), narrow),
            pltpu.VMEM((count, 2, 2, part, share), narrow),
            pltpu.VMEM((count, 2, 2, part, share), narrow),
            pltpu.VMEM((count, 2, 2, part, share), narrow),
            pltpu.VMEM((count, 2, part, share), narrow),
            pltpu.VMEM((count, 2, part, share), full),
            pltpu.VMEM((count, 2, part, share), narrow),
            pltpu.VMEM((count, part, share), narrow),
            pltpu.VMEM((count, part, share), full),
            pltpu.VMEM((count, part, share), narrow),
            pltpu.VMEM((count, part, share), narrow),
            pltpu.VMEM((GROUPS, rows, share), narrow),
            pltpu.VMEM((GROUPS, 2, 2, attend_rows // 2, rank), narrow),
            pltpu.VMEM((GROUPS, 2, 2, attend_rows // 4, 2 * ROPE), narrow),
            pltpu.VMEM((attend_rows, head_cols), narrow),
            pltpu.VMEM((2, 2, attend_rows, 2 * ROPE), narrow),
            pltpu.VMEM((attend_rows, head_cols), narrow),
            pltpu.VMEM((4, attend_rows // 4, width), narrow),
            pltpu.VMEM((2, attend_rows // 4, width), narrow),
            pltpu.VMEM((attend_rows // 4, width), narrow),
            pltpu.VMEM((attend_rows // 4, width), narrow),
            dma((4,)),
            dma((24,)),
        ]
        + [dma((count,))] * 4
        + [dma((2 * count,))] * 4
        + [dma((count,))] * 8
        + [dma((GROUPS,))] * 2
        + [dma((2 * GROUPS,))] * 6
        + [dma((2,))] * 4,
        compiler_params=pltpu.CompilerParams(
            collective_id=0, has_side_effects=True, vmem_limit_bytes=55 * 1024 * 1024
        ),
        cost_estimate=pl.CostEstimate(
            flops=40_000_000_000, bytes_accessed=8_000_000, transcendentals=0
        ),
        name="expert_exchange",
    )(*operands)


def paired(mixer, tokens_b, ffn_gain, route_expert, route_weight, w_gate, w_up, w_down):
    query_latent, key_latent, rope_key, query_gain, key_gain = mixer[:5]
    mixer_args = (
        query_latent,
        key_latent,
        rope_key.T,
        query_gain.reshape(1, -1),
        key_gain.reshape(1, -1),
        *mixer[5:],
    )
    moe_out, mixer_out = expert_exchange(
        tokens_b, ffn_gain, route_expert.T, route_weight.T, w_gate, w_up, w_down, mixer_args
    )
    return (mixer_out, moe_out)


def body(
    query_latent,
    key_latent,
    rope_key,
    query_gain,
    key_gain,
    w_query,
    w_query_rope,
    w_key,
    w_value,
    w_out,
    tokens_b,
    ffn_gain,
    route_expert,
    route_weight,
    w_gate,
    w_up,
    w_down,
):
    mixer = (
        query_latent,
        key_latent,
        rope_key,
        query_gain,
        key_gain,
        w_query,
        w_query_rope,
        w_key,
        w_value,
        w_out,
    )
    experts = (tokens_b, ffn_gain, route_expert, route_weight, w_gate, w_up, w_down)
    if (
        lax.axis_size("ep") == GROUPS * TOPK
        and lax.axis_size("tp") == 4
        and GROUPS == 4
        and tokens_b.shape[0] == GROUPS * 128
        and w_query.shape[1] == 2 * NOPE
    ):
        return paired(mixer, *experts)
    return (mixer_half(*mixer), expert_half(*experts))


def solution(mesh):
    in_specs = (
        P("ep", None),
        P("ep", None),
        P("ep", None),
        P(),
        P(),
        P(None, "tp"),
        P(None, "tp"),
        P(None, "tp"),
        P(None, "tp"),
        P("tp", None),
        P("ep", None),
        P(),
        P("ep", None),
        P("ep", None),
        P("ep", None, "tp"),
        P("ep", None, "tp"),
        P("ep", "tp", None),
    )
    out_specs = (P(("ep", "tp"), None), P("ep", "tp"))
    return jax.shard_map(body, mesh=mesh, in_specs=in_specs, out_specs=out_specs, check_vma=False)
```

time: 90.7 us -> 64.7 us (0.71)
  Pallas kernels: 75.8 us -> 60.4 us
  local copies, waits for them, and re-layouts: 9.71 us -> 3.44 us
  other arithmetic: 2.43 us -> 0 us
  matrix products: 1.55 us -> 0 us
    pallas_call x1, Pallas kernels: 75.8 us -> 60.4 us  [expert_exchange(): pl.pallas_call(expert_kernel, out_shape=(jax.ShapeDtypeStruct((tok_rows,...]
    unnamed x20 -> x2, local copies, waits for them, and re-layouts: 8.94 us -> 3.44 us
    dot_general x2 -> x0, matrix products: 1.55 us -> none  [the longest x1 1.29 us: paired(): lax.dot_general(order, fin, (((0,), (0,)), ((), ())), preferred_element_t...]
    convert_element_type x1 -> x0, other arithmetic: 0.93 us -> none  [paired(): order = hit.astype(jnp.bfloat16)]
where the time goes in v1:
time: 64.7 us; the launch traced here: 64.5 us
  Pallas kernels  60.4 us (93%)
  local copies, waits for them, and re-layouts  3.44 us (5%)
  between operations  0.65 us (1%)
    pallas_call x1, Pallas kernels, expert_exchange(): pl.pallas_call(expert_kernel, out_shape=(jax.ShapeDtypeStruct((tok_rows,...  60.4 us
    unnamed x2, local copies, waits for them, and re-layouts  3.44 us

profile of v1, /device:TPU:0, one launch (start us, length us, event | category | flops | bytes accessed | tf_op | source)
XLA Modules:
  0.0 64.5 jit_solution(6466702004396681745)
XLA Ops:
  0.6 60.4 %expert_exchange.1 = (bf16[512,512]{1,0:T(8,128)(2,1)}, bf16[32,2048]{1,0:T(8,128)(2,1)}) custom-call(bf16[512,2048]{1,0:T(8,128)(2,1)} %tokens_hbm.1, f32[1,2048]{1,0:T(1,128)} %bitcast.7, s32[2,512]{1,0:T(2,128)} %bitcast.8, f32[2,512]{1,0:T(2,128)} %bitcast.9, bf16[1,2048,256]{2,1,0:T(8,128)(2,1)} %gate_hbm.1, bf16[1,2048,256]{2,1,0:T(8,128)(2,1)} %up_hbm.1, ...), custom_call_target="tpu_custom_call" | custom-call | flops 40000000000 | bytes 8000000 | tf_op jit(solution)/shard_map/expert_exchange/pallas_call | solution.py:937
  61.0 1.6 %copy.21 = bf16[32,2048]{1,0:T(8,128)(2,1)} copy(bf16[32,2048]{1,0:T(8,128)(2,1)} %get-tuple-element.8) | data formatting | bytes 262144
  62.6 1.9 %copy.22 = bf16[512,512]{1,0:T(8,128)(2,1)} copy(bf16[512,512]{1,0:T(8,128)(2,1)} %get-tuple-element.9) | data formatting | bytes 1048576

commit v2 on v1

--- a/solution.py
+++ b/solution.py
@@ -16,9 +16,10 @@
 GROUPS = 4
 MESH = pl.DeviceIdType.MESH
 HALVES = 2
-SPARES = (4, 1, 4, 3, 3, 4, 4, 4)
-X_LEADS = (0, 2, 3, 5, 7)
-SENDS = (2, 0, 1, 6, 3, 7, 4, 5)
+Z_SPARES = (1, 1, 3, 2, 4, 4, 4, 4)
+X_SPARES = (1, 1, 4, 2, 4, 4, 4, 4)
+X_LEADS = (0, 1, 4, 6, 7)
+SENDS = (2, 6, 3, 7, 0, 1, 4, 5)
 
 
 epsilon = 1e-06
@@ -315,14 +316,19 @@
     tok_rows = tokens_ref.shape[0]
     share = fin_ref.shape[2]
 
-    def spare_of(u):
-        return half * SPARES[u] // 8
+    def sides(eighths):
+        spare = half * eighths // 8
+        kept = pl.ds(pl.multiple_of(y * spare, 128), half - spare)
+        return kept, pl.ds(pl.multiple_of(y * (half - spare), 128), spare)
 
     def carried(u):
-        return pl.ds(pl.multiple_of(y * spare_of(u), 128), half - spare_of(u))
-
-    def passed(u):
-        return pl.ds(pl.multiple_of(y * (half - spare_of(u)), 128), spare_of(u))
+        return sides(Z_SPARES[u])[0]
+
+    def forwarded(u):
+        return sides(X_SPARES[u])[0]
+
+    def passed(u, rel):
+        return sides((Z_SPARES if rel == 0 else X_SPARES)[u])[1]
 
     at_end = (z == 0) | (z == GROUPS - 1)
 
@@ -344,7 +350,6 @@
         loads[name].start()
 
     load("route", route_hbm, route_ref)
-    load("gain", gain_hbm, gain_ref)
     token_loads = []
     for k in range(4):
         lines = pl.ds(k * (tok_rows // 4), tok_rows // 4)
@@ -352,21 +357,24 @@
             pltpu.make_async_copy(tokens_hbm.at[lines], tokens_ref.at[lines], token_sem.at[k])
         )
         token_loads[k].start()
-    load("share", weight_hbm, share_ref)
-    load("key_gain", key_gain_hbm, key_gain_ref)
-    load("latent", latent_hbm, latent_ref)
-    load("rope", rope_hbm, rope_ref)
-    load("gate", gate_hbm.at[0], gate_ref)
-    load("up", up_hbm.at[0], up_ref)
-    for t in range(4):
-        load(("down", t), down_hbm.at[0, :, pl.ds(t * share, share)], down_ref.at[t])
-    load("query_gain", query_gain_hbm, query_gain_ref)
-    load("query", query_hbm, query_ref)
-    load("w_query", w_query_hbm, w_query_ref)
-    load("w_rope", w_rope_hbm, w_rope_ref)
-    load("w_key", w_key_hbm, w_key_ref)
-    load("w_value", w_value_hbm, w_value_ref)
-    load("w_out", w_out_hbm, w_out_ref)
+    load("gain", gain_hbm, gain_ref)
+
+    def load_rest():
+        load("share", weight_hbm, share_ref)
+        load("gate", gate_hbm.at[0], gate_ref)
+        load("up", up_hbm.at[0], up_ref)
+        for t in range(4):
+            load(("down", t), down_hbm.at[0, :, pl.ds(t * share, share)], down_ref.at[t])
+        load("key_gain", key_gain_hbm, key_gain_ref)
+        load("latent", latent_hbm, latent_ref)
+        load("rope", rope_hbm, rope_ref)
+        load("query_gain", query_gain_hbm, query_gain_ref)
+        load("query", query_hbm, query_ref)
+        load("w_query", w_query_hbm, w_query_ref)
+        load("w_rope", w_rope_hbm, w_rope_ref)
+        load("w_key", w_key_hbm, w_key_ref)
+        load("w_value", w_value_hbm, w_value_ref)
+        load("w_out", w_out_hbm, w_out_ref)
 
     def dot(left, right):
         return jnp.dot(left, right, preferred_element_type=jnp.float32)
@@ -412,24 +420,22 @@
         middle = rest.astype(jnp.bfloat16)
         return wide(top), wide(middle), rest - wide(middle)
 
-    step_rows = 32
-
-    def scale_step(step, unused):
-        lines = pl.ds(pl.multiple_of(step * step_rows, step_rows), step_rows)
-        widened = wide(tokens_ref[lines, :])
-        mean = jnp.mean(widened * widened, axis=-1, keepdims=True)
-        lane = iota((step_rows, 128), 1)
-        table = jnp.zeros((step_rows, 128), jnp.float32)
-        for k, value in enumerate(split(lax.rsqrt(mean + epsilon))):
-            table = jnp.where(lane == k, jnp.broadcast_to(value, table.shape), table)
-        scale_ref[lines, :] = table.astype(jnp.bfloat16)
-        return unused
-
-    per_load = tok_rows // 4 // step_rows
+    width = tokens_ref.shape[1]
     for k in range(4):
         token_loads[k].wait()
-        lax.fori_loop(k * per_load, (k + 1) * per_load, scale_step, 0, unroll=True)
+        lines = slice(k * (tok_rows // 4), (k + 1) * (tok_rows // 4))
+        squares = jnp.zeros((tok_rows // 4, 128), jnp.float32)
+        for j in range(width // 128):
+            widened = wide(tokens_ref[lines, j * 128 : (j + 1) * 128])
+            squares = squares + widened * widened
+        mean = jnp.sum(squares, axis=-1, keepdims=True) * (1.0 / width)
+        lane = iota(squares.shape, 1)
+        table = jnp.zeros(squares.shape, jnp.float32)
+        for j, value in enumerate(split(lax.rsqrt(mean + epsilon))):
+            table = jnp.where(lane == j, jnp.broadcast_to(value, table.shape), table)
+        scale_ref[lines, :] = table.astype(jnp.bfloat16)
     loads["gain"].wait()
+    load_rest()
 
     def remote(source, target, send, recv, peer):
         return pltpu.make_async_remote_copy(
@@ -465,11 +471,11 @@
         )
 
     def x_copy(u):
-        piece = member_ref.at[c, block_at(u), x, lines_at(u), carried(u)]
+        piece = member_ref.at[c, block_at(u), x, lines_at(u), forwarded(u)]
         return remote(piece, piece, x_send.at[u], x_recv.at[u], at_x)
 
     def y_copy(u, rel):
-        piece = member_ref.at[c, block_at(u), line_at(rel), lines_at(u), passed(u)]
+        piece = member_ref.at[c, block_at(u), line_at(rel), lines_at(u), passed(u, rel)]
         k = 2 * u + rel
         return remote(piece, piece, y_send.at[k], y_recv.at[k], at_y)
 
@@ -556,9 +562,9 @@
         return (picked * scale * gain_ref[:, place_of]).astype(jnp.bfloat16)
 
     def make_units(d):
-        spare = min(spare_of(d * HALVES + h) for h in range(HALVES))
-        kept = pl.ds(pl.multiple_of(y * spare, 128), half - spare)
-        outgoing_ref[flip(z, d), :, kept] = permuted(
+        eighths = min(Z_SPARES[d * HALVES + h] for h in range(HALVES))
+        spare = half * eighths // 8
+        outgoing_ref[flip(z, d), :, sides(eighths)[0]] = permuted(
             flip(z, d), scale_of(flip(z, d)), c * half + y * spare, half - spare
         )
 
@@ -802,14 +808,16 @@
     def from_z(u):
         arrive(z_copy, u)
         start(x_copy, u)
-        start(y_copy, u, 0)
+        if Z_SPARES[u] > 0:
+            start(y_copy, u, 0)
 
     def from_x(u):
         arrive(x_copy, u)
         start(y_copy, u, 1)
 
     def from_y(u, rel):
-        arrive(y_copy, u, rel)
+        if rel == 1 or Z_SPARES[u] > 0:
+            arrive(y_copy, u, rel)
         start(c_copy, u, rel)
 
     def gathered(u):
@@ -834,22 +842,17 @@
     def from_kc(d):
         arrive(kc_copy, d)
 
-    def back_term(d):
-        return dot(back_ref[flip(z, d)], fin_ref[flip(z, d)])
-
-    def returned(u):
-        arrive(o_copy, u)
-
-    def back_early():
-        for d in (1, 3):
+    added = []
+
+    def give_back(d):
+        if d > 0:
             for h in range(HALVES):
-                returned(d * HALVES + h)
-        moe_ref[...] = (back_term(0) + back_term(1) + back_term(3)).astype(jnp.bfloat16)
-
-    def back_last():
-        for h in range(HALVES):
-            returned(2 * HALVES + h)
-        moe_ref[...] = (wide(moe_ref[...]) + back_term(2)).astype(jnp.bfloat16)
+                arrive(o_copy, d * HALVES + h)
+        term = dot(back_ref[flip(z, d)], fin_ref[flip(z, d)])
+        if added:
+            term = term + wide(moe_ref[...])
+        added.append(d)
+        moe_ref[...] = term.astype(jnp.bfloat16)
 
     steps = {
         "z": from_z,
@@ -871,8 +874,7 @@
         "attend": attend,
         "join": attend_join,
         "last": attend_last,
-        "early": back_early,
-        "final": back_last,
+        "b": give_back,
     }
 
     for item in SCHEDULE:
@@ -894,18 +896,18 @@
 
 
 SCHEDULE = (
-    "keys", "loaded", "<x.1", "z.2", "back", "x.0", "z.3", ">y.0.1", ">x.1", ">z.6", ">kz.1", "x.2",
-    ">y.2.0", ">x.3", ">y.6.0", "z.7", "kx.0", ">y.1.1", "<z.6", "<y.2.0", "<y.0.1", "g.0", "m.0",
-    ">kc.0", ">z.5", ">kx.1", "<x.3", "<y.1.1", "weights", "<kz.3", "<y.2.1", "<z.4", "<x.6",
-    "<y.3.1", "<z.5", "<x.7", "<y.6.0", "<kz.1", "<y.3.0", "<y.4.0", "<y.6.1", "1.0", ">z.4", "g.1",
-    "m.1", ">x.6", ">y.2.1", "<kz.2", "<x.5", "y.7.0", ">x.7", "g.2", "m.2", ">kz.2", ">y.3.0",
-    ">x.5", ">y.5.0", ">y.3.1", "columns.2", "columns.1", ">y.6.1", ">y.4.0", ">kz.3", "<kc.0",
-    "<kx.1", "<y.5.0", "<y.7.1", "1.1", "columns.0", "<x.4", "1.2", "g.3", "m.3", "g.6", "m.6",
-    ">y.5.1", ">x.4", "1.3", "<kx.2", "<kc.1", "<kx.3", "<y.5.1", "1.6", ">y.7.1", ">kx.3", ">kx.2",
-    ">kc.1", ">kc.2", "g.5", "m.5", ">y.4.1", "2.1", "2.2", "<kc.3", "<y.4.1", "g.7", "m.7", "1.5",
-    "2.0", "2.3", "g.4", "m.4", ">kc.3", "2.6", "<kc.2", "3.1", "1.4", "columns.3", "1.7", "3.2",
-    "attend", "2.5", "3.0", "3.6", "3.3", "join", "2.4", "2.7", "3.5", "3.4", "3.7", "last",
-    "early", "final",
+    "z.2", "<z.7", "x.0", "<z.6", "<x.1", "<y.2.0", "z.3", "<y.1.1", "y.0.1", ">x.1", ">z.6",
+    ">x.2", "keys", "<x.6", "<x.2", "z.4", "<kz.1", "loaded", ">y.1.1", ">z.7", "g.0", "m.0",
+    "<z.5", "<y.6.1", "weights", ">z.5", ">y.2.1", "g.1", "m.1", ">x.6", ">kz.1", ">y.2.0", "<x.3",
+    "<x.4", "<y.2.1", "<kz.3", "<kz.2", "1.0", ">x.3", "<y.5.0", "<y.6.0", "<x.7", "<y.7.0",
+    "<y.4.0", "g.2", "m.2", ">y.3.0", ">y.6.0", "x.5", ">y.4.0", ">y.6.1", ">x.4", ">kz.2", "1.2",
+    ">y.5.0", ">kz.3", ">y.7.0", ">kx.0", "<y.4.1", "<kx.2", "y.3.1", "columns.0", "1.1", "g.6",
+    "m.6", ">kx.2", "2.0", "columns.2", "y.5.1", ">x.7", ">y.4.1", "1.6", "g.5", "m.5", "<y.3.0",
+    "g.4", "m.4", "<y.7.1", "2.2", "<kc.2", "<kx.0", "<kx.3", "columns.3", "1.5", ">kx.1", "g.3",
+    "m.3", ">kc.2", "3.0", "1.4", "<kc.0", "back", ">kc.0", ">y.7.1", "2.6", "1.3", "g.7", "m.7",
+    ">kc.1", ">kx.3", "columns.1", "<kx.1", "2.5", "3.2", "<kc.3", "1.7", "2.1", "3.6", "2.4",
+    "<kc.1", "3.5", ">kc.3", "attend", "3.1", "3.4", "2.7", "2.3", "join", "3.7", "3.3", "b.2",
+    "b.0", "last", "b.1", "b.3",
 )
 
 
@@ -937,8 +939,8 @@
     return pl.pallas_call(
         expert_kernel,
         out_shape=(
-            jax.ShapeDtypeStruct((tok_rows, share), narrow),
-            jax.ShapeDtypeStruct((attend_rows // 4, width), narrow),
+            pltpu.VMEM((tok_rows, share), narrow),
+            pltpu.VMEM((attend_rows // 4, width), narrow),
         ),
         in_specs=[anywhere] * len(operands),
         out_specs=(vmem, vmem),
@@ -998,13 +1000,13 @@
         + [dma((2 * GROUPS,))] * 6
         + [dma((2,))] * 4,
         compiler_params=pltpu.CompilerParams(
-            collective_id=0, has_side_effects=True, vmem_limit_bytes=55 * 1024 * 1024
+            collective_id=0, has_side_effects=True, vmem_limit_bytes=48 * 1024 * 1024
         ),
         cost_estimate=pl.CostEstimate(
             flops=40_000_000_000, bytes_accessed=8_000_000, transcendentals=0
         ),
         name="expert_exchange",
-    )(*operands)
+    )(*(pltpu.with_memory_space_constraint(operand, pltpu.HBM) for operand in operands))
 
 
 def paired(mixer, tokens_b, ffn_gain, route_expert, route_weight, w_gate, w_up, w_down):

time: 64.7 us -> 58.5 us (0.904)
  Pallas kernels: 60.4 us -> 56.2 us
  local copies, waits for them, and re-layouts: 3.44 us -> 1.45 us
    pallas_call x1, Pallas kernels: 60.4 us -> 56.2 us  [expert_exchange(): pl.pallas_call(expert_kernel, out_shape=(pltpu.VMEM((tok_rows, share), na...]
    unnamed x2, local copies, waits for them, and re-layouts: 3.44 us -> 1.45 us
where the time goes in v2:
time: 58.5 us; the launch traced here: 58.3 us
  Pallas kernels  56.2 us (96%)
  local copies, waits for them, and re-layouts  1.45 us (2%)
  between operations  0.65 us (1%)
    pallas_call x1, Pallas kernels, expert_exchange(): pl.pallas_call(expert_kernel, out_shape=(pltpu.VMEM((tok_rows, share), na...  56.2 us
    unnamed x2, local copies, waits for them, and re-layouts  1.45 us

profile of v2, /device:TPU:0, one launch (start us, length us, event | category | flops | bytes accessed | tf_op | source)
XLA Modules:
  0.0 58.3 jit_solution(4738494384492868910)
XLA Ops:
  0.6 56.2 %expert_exchange.1 = (bf16[512,512]{1,0:T(8,128)(2,1)S(1)}, bf16[32,2048]{1,0:T(8,128)(2,1)S(1)}) custom-call(bf16[512,2048]{1,0:T(8,128)(2,1)} %tokens_hbm.1, f32[1,2048]{1,0:T(1,128)} %bitcast.7, s32[2,512]{1,0:T(2,128)} %bitcast.8, f32[2,512]{1,0:T(2,128)} %bitcast.9, bf16[1,2048,256]{2,1,0:T(8,128)(2,1)} %gate_hbm.1, bf16[1,2048,256]{2,1,0:T(8,128)(2,1)} %up_hbm.1, ...), custom_call_target="tpu_custom_call" | custom-call | flops 40000000000 | bytes 8000000 | tf_op jit(solution)/shard_map/expert_exchange/pallas_call | solution.py:939
  56.9 0.7 %copy.21 = bf16[32,2048]{1,0:T(8,128)(2,1)} copy(bf16[32,2048]{1,0:T(8,128)(2,1)S(1)} %get-tuple-element.6) | data formatting | bytes 262144
  57.5 0.8 %copy.22 = bf16[512,512]{1,0:T(8,128)(2,1)} copy(bf16[512,512]{1,0:T(8,128)(2,1)S(1)} %get-tuple-element.7) | data formatting | bytes 1048576

commit v3 on v2

--- a/solution.py
+++ b/solution.py
@@ -16,10 +16,10 @@
 GROUPS = 4
 MESH = pl.DeviceIdType.MESH
 HALVES = 2
-Z_SPARES = (1, 1, 3, 2, 4, 4, 4, 4)
-X_SPARES = (1, 1, 4, 2, 4, 4, 4, 4)
-X_LEADS = (0, 1, 4, 6, 7)
-SENDS = (2, 6, 3, 7, 0, 1, 4, 5)
+Z_SPARES = (3, 3, 3, 3, 4, 3, 4, 4)
+X_SPARES = (3, 3, 3, 3, 4, 3, 4, 4)
+X_LEADS = (1, 4, 5, 6, 7)
+SENDS = (2, 6, 3, 0, 1, 7, 4, 5)
 
 
 epsilon = 1e-06
@@ -896,18 +896,18 @@
 
 
 SCHEDULE = (
-    "z.2", "<z.7", "x.0", "<z.6", "<x.1", "<y.2.0", "z.3", "<y.1.1", "y.0.1", ">x.1", ">z.6",
-    ">x.2", "keys", "<x.6", "<x.2", "z.4", "<kz.1", "loaded", ">y.1.1", ">z.7", "g.0", "m.0",
-    "<z.5", "<y.6.1", "weights", ">z.5", ">y.2.1", "g.1", "m.1", ">x.6", ">kz.1", ">y.2.0", "<x.3",
-    "<x.4", "<y.2.1", "<kz.3", "<kz.2", "1.0", ">x.3", "<y.5.0", "<y.6.0", "<x.7", "<y.7.0",
-    "<y.4.0", "g.2", "m.2", ">y.3.0", ">y.6.0", "x.5", ">y.4.0", ">y.6.1", ">x.4", ">kz.2", "1.2",
-    ">y.5.0", ">kz.3", ">y.7.0", ">kx.0", "<y.4.1", "<kx.2", "y.3.1", "columns.0", "1.1", "g.6",
-    "m.6", ">kx.2", "2.0", "columns.2", "y.5.1", ">x.7", ">y.4.1", "1.6", "g.5", "m.5", "<y.3.0",
-    "g.4", "m.4", "<y.7.1", "2.2", "<kc.2", "<kx.0", "<kx.3", "columns.3", "1.5", ">kx.1", "g.3",
-    "m.3", ">kc.2", "3.0", "1.4", "<kc.0", "back", ">kc.0", ">y.7.1", "2.6", "1.3", "g.7", "m.7",
-    ">kc.1", ">kx.3", "columns.1", "<kx.1", "2.5", "3.2", "<kc.3", "1.7", "2.1", "3.6", "2.4",
-    "<kc.1", "3.5", ">kc.3", "attend", "3.1", "3.4", "2.7", "2.3", "join", "3.7", "3.3", "b.2",
-    "b.0", "last", "b.1", "b.3",
+    ">z.2", ">x.0", "loaded", "<z.6", "<x.0", "<z.7", "<z.2", "<x.6", "<z.3", "<x.2", "<y.2.0",
+    "<y.7.0", "<y.6.1", "x.1", ">z.6", ">z.3", ">y.1.1", "y.0.1", ">z.4", ">x.6", ">z.7", "y.6.0",
+    "<x.3", "keys", ">z.5", ">y.6.1", "x.7", "<z.4", "g.6", "m.6", ">x.3", ">y.7.0", ">x.4",
+    ">y.3.0", ">kz.1", "<z.5", "<y.3.1", "g.0", "m.0", ">kx.0", ">x.5", "<y.1.1", "<kz.1", "1.6",
+    "<kz.3", "<y.3.0", "<y.7.1", "<kx.0", "<y.2.1", "weights", ">y.7.1", ">x.2", ">kz.2", ">y.5.0",
+    ">kz.3", ">y.3.1", ">kx.1", "<x.4", "<x.5", "g.7", "m.7", "1.0", "<y.5.0", "<kz.2", "<y.4.0",
+    "<kc.0", "<kx.1", "<y.4.1", "g.1", "m.1", ">kc.0", ">y.5.1", ">y.4.1", "1.7", "<y.5.1",
+    "columns.3", ">y.4.0", "g.3", "m.3", "2.6", ">y.2.1", "columns.2", "g.5", "m.5", ">kx.2",
+    ">y.2.0", "1.3", "g.4", "m.4", "1.5", "g.2", "m.2", "back", "3.6", "2.7", "<kc.1", "<kx.2",
+    "1.4", "columns.1", "2.3", ">kx.3", "2.5", "1.2", "kc.2", "1.1", ">kc.3", ">kc.1", "<kx.3",
+    "3.7", "<kc.3", "attend", "3.5", "2.4", "2.0", "columns.0", "3.3", "join", "2.2", "3.4", "3.0",
+    "2.1", "b.3", "3.2", "3.1", "last", "b.0", "b.2", "b.1",
 )
 
 

time: 58.5 us -> 58.4 us (level)
  no operation moved by 1% of the time
where the time goes in v3:
time: 58.4 us; the launch traced here: 58.3 us
  Pallas kernels  56.2 us (96%)
  local copies, waits for them, and re-layouts  1.45 us (2%)
  between operations  0.65 us (1%)
    pallas_call x1, Pallas kernels, expert_exchange(): pl.pallas_call(expert_kernel, out_shape=(pltpu.VMEM((tok_rows, share), na...  56.2 us
    unnamed x2, local copies, waits for them, and re-layouts  1.45 us

profile of v3, /device:TPU:0, one launch (start us, length us, event | category | flops | bytes accessed | tf_op | source)
XLA Modules:
  0.0 58.3 jit_solution(12075322074498721794)
XLA Ops:
  0.6 56.2 %expert_exchange.1 = (bf16[512,512]{1,0:T(8,128)(2,1)S(1)}, bf16[32,2048]{1,0:T(8,128)(2,1)S(1)}) custom-call(bf16[512,2048]{1,0:T(8,128)(2,1)} %tokens_hbm.1, f32[1,2048]{1,0:T(1,128)} %bitcast.7, s32[2,512]{1,0:T(2,128)} %bitcast.8, f32[2,512]{1,0:T(2,128)} %bitcast.9, bf16[1,2048,256]{2,1,0:T(8,128)(2,1)} %gate_hbm.1, bf16[1,2048,256]{2,1,0:T(8,128)(2,1)} %up_hbm.1, ...), custom_call_target="tpu_custom_call" | custom-call | flops 40000000000 | bytes 8000000 | tf_op jit(solution)/shard_map/expert_exchange/pallas_call | solution.py:939
  56.8 0.7 %copy.21 = bf16[32,2048]{1,0:T(8,128)(2,1)} copy(bf16[32,2048]{1,0:T(8,128)(2,1)S(1)} %get-tuple-element.6) | data formatting | bytes 262144
  57.5 0.8 %copy.22 = bf16[512,512]{1,0:T(8,128)(2,1)} copy(bf16[512,512]{1,0:T(8,128)(2,1)S(1)} %get-tuple-element.7) | data formatting | bytes 1048576

commit v4 on v2

--- a/solution.py
+++ b/solution.py
@@ -16,9 +16,9 @@
 GROUPS = 4
 MESH = pl.DeviceIdType.MESH
 HALVES = 2
-Z_SPARES = (1, 1, 3, 2, 4, 4, 4, 4)
-X_SPARES = (1, 1, 4, 2, 4, 4, 4, 4)
-X_LEADS = (0, 1, 4, 6, 7)
+Z_SPARES = (0, 1, 4, 3, 4, 4, 4, 4)
+X_SPARES = (3, 1, 4, 3, 4, 4, 4, 4)
+X_LEADS = (1, 3, 4, 6)
 SENDS = (2, 6, 3, 7, 0, 1, 4, 5)
 
 
@@ -896,18 +896,18 @@
 
 
 SCHEDULE = (
-    "z.2", "<z.7", "x.0", "<z.6", "<x.1", "<y.2.0", "z.3", "<y.1.1", "y.0.1", ">x.1", ">z.6",
-    ">x.2", "keys", "<x.6", "<x.2", "z.4", "<kz.1", "loaded", ">y.1.1", ">z.7", "g.0", "m.0",
-    "<z.5", "<y.6.1", "weights", ">z.5", ">y.2.1", "g.1", "m.1", ">x.6", ">kz.1", ">y.2.0", "<x.3",
-    "<x.4", "<y.2.1", "<kz.3", "<kz.2", "1.0", ">x.3", "<y.5.0", "<y.6.0", "<x.7", "<y.7.0",
-    "<y.4.0", "g.2", "m.2", ">y.3.0", ">y.6.0", "x.5", ">y.4.0", ">y.6.1", ">x.4", ">kz.2", "1.2",
-    ">y.5.0", ">kz.3", ">y.7.0", ">kx.0", "<y.4.1", "<kx.2", "y.3.1", "columns.0", "1.1", "g.6",
-    "m.6", ">kx.2", "2.0", "columns.2", "y.5.1", ">x.7", ">y.4.1", "1.6", "g.5", "m.5", "<y.3.0",
-    "g.4", "m.4", "<y.7.1", "2.2", "<kc.2", "<kx.0", "<kx.3", "columns.3", "1.5", ">kx.1", "g.3",
-    "m.3", ">kc.2", "3.0", "1.4", "<kc.0", "back", ">kc.0", ">y.7.1", "2.6", "1.3", "g.7", "m.7",
-    ">kc.1", ">kx.3", "columns.1", "<kx.1", "2.5", "3.2", "<kc.3", "1.7", "2.1", "3.6", "2.4",
-    "<kc.1", "3.5", ">kc.3", "attend", "3.1", "3.4", "2.7", "2.3", "join", "3.7", "3.3", "b.2",
-    "b.0", "last", "b.1", "b.3",
+    "keys", "loaded", "<z.2", "<z.6", "x.0", "<z.7", "<x.1", "<x.2", "<y.7.0", "z.3", "<x.6",
+    "y.0.1", ">x.1", ">z.6", ">z.2", "<x.7", "<y.2.1", "<y.6.0", "x.3", ">x.6", ">kz.1", ">z.7",
+    "<y.6.1", "z.4", ">x.7", ">y.6.1", ">y.7.0", ">y.6.0", "<y.7.1", "z.5", "g.0", "m.0", ">y.3.1",
+    ">x.4", "g.6", "m.6", ">y.7.1", "<kz.1", "<y.4.0", "<x.4", "weights", "<kz.3", "<y.3.1",
+    "<y.3.0", "x.5", ">y.3.0", ">kz.2", "<y.2.0", "1.6", ">kx.1", "g.7", "m.7", ">x.2", "<y.5.0",
+    "g.3", "m.3", ">kx.2", "<y.1.1", "1.7", ">y.5.0", ">y.4.0", ">kz.3", "y.5.1", ">y.2.0", "y.4.1",
+    "1.3", "columns.3", "g.5", "m.5", ">kc.2", "2.6", "columns.1", ">y.2.1", "<kx.3", "1.5",
+    ">kx.3", "<kx.1", "g.4", "m.4", "columns.0", "<kc.3", "2.7", "g.2", "m.2", ">kx.0", "<kz.2",
+    "<kc.1", "3.6", "2.3", "1.4", "columns.2", "<kx.0", "1.2", ">y.1.1", "<kc.0", "3.7", ">kc.3",
+    ">kc.1", "<kx.2", "g.1", "m.1", "2.5", "1.0", ">kc.0", "3.3", "<kc.2", "attend", "2.2", "1.1",
+    "3.5", "2.4", "join", "3.2", "3.4", "2.0", "back", "b.3", "2.1", "last", "3.0", "b.1", "3.1",
+    "b.0", "b.2",
 )
 
 

time: 58.5 us -> 57.5 us (0.983)
  Pallas kernels: 56.2 us -> 55.2 us
    pallas_call x1, Pallas kernels: 56.2 us -> 55.2 us  [expert_exchange(): pl.pallas_call(expert_kernel, out_shape=(pltpu.VMEM((tok_rows, share), na...]
where the time goes in v4:
time: 57.5 us; the launch traced here: 57.3 us
  Pallas kernels  55.2 us (96%)
  local copies, waits for them, and re-layouts  1.45 us (3%)
  between operations  0.65 us (1%)
    pallas_call x1, Pallas kernels, expert_exchange(): pl.pallas_call(expert_kernel, out_shape=(pltpu.VMEM((tok_rows, share), na...  55.2 us
    unnamed x2, local copies, waits for them, and re-layouts  1.45 us

profile of v4, /device:TPU:0, one launch (start us, length us, event | category | flops | bytes accessed | tf_op | source)
XLA Modules:
  0.0 57.3 jit_solution(12611812964599193559)
XLA Ops:
  0.6 55.2 %expert_exchange.1 = (bf16[512,512]{1,0:T(8,128)(2,1)S(1)}, bf16[32,2048]{1,0:T(8,128)(2,1)S(1)}) custom-call(bf16[512,2048]{1,0:T(8,128)(2,1)} %tokens_hbm.1, f32[1,2048]{1,0:T(1,128)} %bitcast.7, s32[2,512]{1,0:T(2,128)} %bitcast.8, f32[2,512]{1,0:T(2,128)} %bitcast.9, bf16[1,2048,256]{2,1,0:T(8,128)(2,1)} %gate_hbm.1, bf16[1,2048,256]{2,1,0:T(8,128)(2,1)} %up_hbm.1, ...), custom_call_target="tpu_custom_call" | custom-call | flops 40000000000 | bytes 8000000 | tf_op jit(solution)/shard_map/expert_exchange/pallas_call | solution.py:939
  55.9 0.7 %copy.21 = bf16[32,2048]{1,0:T(8,128)(2,1)} copy(bf16[32,2048]{1,0:T(8,128)(2,1)S(1)} %get-tuple-element.6) | data formatting | bytes 262144
  56.5 0.8 %copy.22 = bf16[512,512]{1,0:T(8,128)(2,1)} copy(bf16[512,512]{1,0:T(8,128)(2,1)S(1)} %get-tuple-element.7) | data formatting | bytes 1048576
